TPU v7x, 32 devices: a whole 2x2x4 slice. The times are simulated.
32 devices in a mesh: sp: 8 (over z, y), tp: 4 (over x, core).
Axes of the slice: x: 2, y: 2, z: 4, core: 2. Of those that a mesh axis runs over, the one named last changes fastest.
Arguments:
- activations: bfloat16 [3584, 2048], P(('sp', 'tp')), may hold values from -27.5 to 27.5
- query_weight: bfloat16 [2048, 2048], P(None, 'tp'), may hold values from -0.088388348 to 0.088388348
- key_weight: bfloat16 [2048, 2048], P(None, 'tp'), may hold values from -0.088388348 to 0.088388348
- value_weight: bfloat16 [2048, 2048], P(None, 'tp'), may hold values from -0.125 to 0.125
- out_weight: bfloat16 [2048, 2048], P('tp'), may hold values from -0.125 to 0.125
- lambdas: float32 [8], P('tp'), may hold values from 0.3 to 0.8
- head_gain: float32 [256], replicated, may hold values from 0.1 to 1.9
Outputs:
- mixed: bfloat16 [3584, 2048], P(('sp', 'tp'))
All inputs are finite; a program needn't handle non-finite values.
Results may differ from a plain program's by a relative error of at most 0.014.
Values may be sent and summed in bfloat16 or wider, within the bound.
A program may use at most 128 MiB of HBM per device.

v0:
```python
import functools
import math

import jax
import jax.numpy as jnp
from jax import lax
from jax.experimental import pallas as pl
from jax.experimental.pallas import tpu as pltpu
from jax.sharding import PartitionSpec as P

HEAD = 128
VALUE = 256


norm_floor = 0.02
very_low = -1e30
MESH = pl.DeviceIdType.MESH


def layer_kernel(
    S, T, L, R,
    act, qw, kw, vw, ow, lam_in, gain,
    out,
    A, WP, W, PR, PC, KV, HO, HI, LS, LB, ACC, MX, DN, TOT,
    w_sem, own_sem, a_send, a_recv, lam_send, lam_recv, o_send, o_recv, m_send, m_recv,
    p_send, p_recv, f_send, f_recv, h_send, h_recv,
):
    X, Y = 2, 2
    Z = S // Y
    H = Z // 2
    s = lax.axis_index("sp")
    t = lax.axis_index("tp")
    x = t // 2
    c = t % 2
    y = s % Y
    z = s // Y
    mate = x * 2 + (1 - c)
    across = (1 - x) * 2 + c
    beside = z * Y + (1 - y)
    upper = z // (Z // 2)
    near = upper * (Z // 2)
    head = x * 2 * L + z
    span = T * R
    scale = HEAD ** (-0.5) * math.log2(math.e)

    def remote(src, dst, ss, rs, sp, tp):
        return pltpu.make_async_remote_copy(
            src_ref=src, dst_ref=dst, send_sem=ss, recv_sem=rs,
            device_id=(sp, tp), device_id_type=MESH,
        )

    def weight_copy(k):
        return pltpu.make_async_copy((qw, kw, vw)[k], WP.at[k], w_sem.at[k])

    def own_act():
        return pltpu.make_async_copy(act, A.at[t], own_sem.at[0])

    def own_ow():
        return pltpu.make_async_copy(ow, W.at[pl.ds(t * L, L)], own_sem.at[1])

    def act_across():
        return remote(act, A.at[t], a_send.at[0], a_recv.at[t], s, across)

    def act_mate():
        return remote(act, A.at[t], a_send.at[1], a_recv.at[t], s, mate)

    def act_pass():
        return remote(A.at[across], A.at[across], a_send.at[2], a_recv.at[across], s, mate)

    def wait_act(i):
        remote(act, A.at[i], a_send.at[0], a_recv.at[i], s, mate).wait_recv()

    def quarter(owner, q):
        rows = pl.ds(pl.multiple_of((q % 2) * (VALUE // 2), VALUE // 2), VALUE // 2)
        return owner * L + q // 2, rows

    def turn(j, row):
        return row * (2 * L - 1) if j == 0 else j

    def ow_across(j):
        q = turn(j, y)
        place, rows = quarter(t, q)
        return remote(
            ow.at[q // 2, rows], W.at[place, rows], o_send.at[j], o_recv.at[j], s, across
        )

    def ow_mate():
        return remote(ow, W.at[pl.ds(t * L, L)], m_send.at[0], m_recv.at[0], s, mate)

    last = 2 * L - 1

    cut = VALUE // 2 // H

    def ow_beside(k, row):
        q = turn(0, row)
        first = pl.multiple_of((q % 2) * (VALUE // 2) + k * cut, cut)
        part = W.at[across * L + q // 2, pl.ds(first, cut)]
        return remote(part, part, o_send.at[last + k], o_recv.at[last + k], beside, t)

    def ow_pass(j):
        q = turn(0, 1 - y) if j == last else turn(j, y)
        place, rows = quarter(across, q)
        part = W.at[place, rows]
        return remote(part, part, m_send.at[1 + j], m_recv.at[1 + j], s, mate)

    def lam_out():
        return remote(LS, LB, lam_send.at[0], lam_recv.at[0], s, mate)

    barrier = pltpu.get_barrier_semaphore()
    greeted = [(beside, t)]
    for i in range(Z):
        row = ((z + i) % Z) * Y + y
        greeted += [(row, mate), (row, across)] + ([(row, t)] if i > 0 else [])
    for sp, tp in greeted:
        pl.semaphore_signal(barrier, inc=1, device_id=(sp, tp), device_id_type=MESH)
    weight_copies = [weight_copy(k) for k in range(3)]
    for copy in weight_copies:
        copy.start()
    own_act().start()
    own_ow().start()
    pl.semaphore_wait(barrier, len(greeted))

    for l in range(L):
        LS[l] = jnp.full((8, 128), lam_in[l], jnp.float32)
    act_across().start()
    act_mate().start()
    for j in range(last):
        ow_across(j).start()

    def piece_sp(l):
        return (c * L + l) * Y + y

    def piece(l, xx, d):
        return remote(
            PR.at[l, xx, d], PC.at[z, xx], p_send.at[l, xx, d], p_recv.at[z, xx],
            piece_sp(l), x * 2 + d,
        )

    def stays(l, d):
        return (piece_sp(l) == s) & (c == d)

    def send_piece(l, xx, d):
        @pl.when(stays(l, d))
        def _():
            pltpu.make_async_copy(PR.at[l, xx, d], PC.at[z, xx], p_recv.at[z, xx]).start()

        @pl.when(jnp.logical_not(stays(l, d)))
        def _():
            piece(l, xx, d).start()

    def project(xx):
        rows = A[pl.ds(xx * 2, 2)].reshape(2 * R, A.shape[2])
        for part in range(3):
            got = jnp.dot(rows, WP[part], preferred_element_type=jnp.float32)
            if part == 0:
                got = got * scale
            got = got.astype(jnp.bfloat16)
            for l in range(L):
                cols = got[:, l * 256:(l + 1) * 256]
                PR[l, xx, :, :, part * 256:(part + 1) * 256] = cols.reshape(2, R, 256)
        for i in range(L):
            l = upper * i + (1 - upper) * (L - 1 - i)
            for d in range(2):
                send_piece(l, xx, d)

    own_act().wait()
    for k in range(3):
        weight_copy(k).wait()
    wait_act(mate)
    project(x)
    lam_out().start()
    wait_act(across)
    act_pass().start()
    wait_act((1 - x) * 2 + (1 - c))
    project(1 - x)

    def kv_rows(row, zs, xx, core):
        return pl.ds(((zs * Y + row) * T + xx * 2 + core) * R, R)

    def kv_part(zs, xx):
        return PC.at[zs, xx, :, 256:768]

    def to_beside(zs, xx):
        return remote(
            kv_part(zs, xx), KV.at[kv_rows(y, zs, xx, c)],
            f_send.at[0, zs, xx], f_recv.at[0, zs, xx], beside, t,
        )

    def to_mate(zs, xx):
        return remote(
            kv_part(zs, xx), KV.at[kv_rows(y, zs, xx, c)],
            f_send.at[1, zs, xx], f_recv.at[1, zs, xx], s, mate,
        )

    def to_mate_again(zs, xx):
        part = KV.at[kv_rows(1 - y, zs, xx, c)]
        return remote(part, part, f_send.at[2, zs, xx], f_recv.at[2, zs, xx], s, mate)

    def to_self(zs, xx):
        return pltpu.make_async_copy(
            kv_part(zs, xx), KV.at[kv_rows(y, zs, xx, c)], f_recv.at[3, zs, xx]
        )

    def place(i):
        return (near + i) % Z, (x + i // Z) % X

    def forward(i):
        zs, xx = place(i)
        remote(PR.at[0, 0, 0], PC.at[zs, xx], p_send.at[0, 0, 0], p_recv.at[zs, xx], s, mate).wait_recv()
        to_beside(zs, xx).start()
        to_mate(zs, xx).start()
        to_self(zs, xx).start()

    def relay(i):
        zs, xx = place(i)
        to_beside(zs, xx).wait_recv()
        to_mate_again(zs, xx).start()

    def spread(first, count, weights):
        def both(i, carry):
            forward(first + i)
            if weights:
                @pl.when(i == 0)
                def _():
                    ow_across(0).wait_recv()

                ow_beside(i, y).start()

            @pl.when(i > 0)
            def _():
                relay(first + i - 1)

            return carry

        lax.fori_loop(0, count, both, 0)
        relay(first + count - 1)

    def wait_plane(zs):
        for xx in range(X):
            to_self(zs, xx).wait()
            to_mate(zs, xx).wait_recv()
            to_mate_again(zs, xx).wait_recv()

    q_rows = X * R
    k_rows = Y * span

    def chunk(i, j, masked):
        for m in range(2):
            q = PC[i, :, :, m * 128:(m + 1) * 128].reshape(q_rows, 128)
            keys = KV[pl.ds(j * k_rows, k_rows), m * 128:(m + 1) * 128]
            sc = lax.dot_general(
                q, keys, (((1,), (1,)), ((), ())), preferred_element_type=jnp.float32
            )
            if masked:
                row = lax.broadcasted_iota(jnp.int32, (q_rows, 1), 0)
                col = lax.broadcasted_iota(jnp.int32, (q_rows, k_rows), 1)
                pos = row + jnp.where(row >= R, R, 0) + (y * span + c * R)
                sc = jnp.where(col <= pos, sc, very_low)
            old = MX[i, m, :, :1]
            new = jnp.maximum(old, jnp.max(sc, axis=1, keepdims=True))
            p = jnp.exp2(sc - new)
            factor = jnp.exp2(old - new)
            total = DN[i, m, :, :1] * factor + jnp.sum(p, axis=1, keepdims=True)
            values = KV[pl.ds(j * k_rows, k_rows), 256:512]
            got = jnp.dot(p.astype(jnp.bfloat16), values, preferred_element_type=jnp.float32)
            ACC[i, m] = ACC[i, m] * factor + got
            MX[i, m] = jnp.broadcast_to(new, MX.shape[2:])
            DN[i, m] = jnp.broadcast_to(total, DN.shape[2:])

    def chunks(i, low, high, diagonal):
        def inner(j, carry):
            chunk(i, j, False)
            return carry

        lax.fori_loop(low, high, inner, 0)

        @pl.when(diagonal)
        def _():
            chunk(i, i, True)

    def home(zs, xx):
        return remote(
            HO.at[zs, xx], HI.at[head], h_send.at[zs, xx], h_recv.at[head],
            zs * Y + y, xx * 2 + c,
        )

    def ends_here(zs, xx):
        return (zs == z) & (xx == x)

    def finish(i):
        mine = jnp.where(z // L == c, LS[z % L], LB[z % L])[:1, :1]
        comb = ACC[i, 0] / DN[i, 0, :, :1] - mine * (ACC[i, 1] / DN[i, 1, :, :1])
        inv = lax.rsqrt(jnp.mean(comb * comb, axis=1, keepdims=True) + norm_floor)
        HO[i] = (comb * inv * gain[...]).astype(jnp.bfloat16).reshape(X, R, VALUE)
        for k in range(X):
            xx = (x + 1 + k) % X

            @pl.when(ends_here(i, xx))
            def _():
                pltpu.make_async_copy(HO.at[i, xx], HI.at[head], h_recv.at[head]).start()

            @pl.when(jnp.logical_not(ends_here(i, xx)))
            def _():
                home(i, xx).start()

    MX[...] = jnp.full(MX.shape, very_low, jnp.float32)
    DN[...] = jnp.zeros(DN.shape, jnp.float32)
    ACC[...] = jnp.zeros(ACC.shape, jnp.float32)
    spread(0, Z + H, False)
    lam_out().wait_recv()
    for i in range(H):
        wait_plane(near + i)

    def step(k, carry):
        @pl.when(k == H)
        def _():
            spread(Z + H, H, True)
            ow_mate().start()
            for i in range(H):
                wait_plane((near + H + i) % Z)

        @pl.when(k == Z - 1)
        def _():
            ow_pass(0).start()
            for j in range(1, last - 1):
                ow_across(j).wait_recv()
                ow_pass(j).start()

        early = k < H
        i = jnp.where(early, near + k, jnp.where(upper == 1, k - H, Z - 1 - (k - H)))
        partial = (upper == 1) & (i >= H)
        low = jnp.where(early, near, 0)
        high = jnp.where(partial & jnp.logical_not(early), H, i)
        used = (upper == 1) | (k < Z)

        @pl.when(used)
        def _():
            chunks(i, low, high, jnp.logical_not(partial) | early)

            @pl.when(jnp.logical_not(partial & early))
            def _():
                finish(i)

        return carry

    lax.fori_loop(0, Z + H, step, 0)

    own_ow().wait()
    ow_mate().wait_recv()
    for i in range(H):
        ow_beside(i, 1 - y).wait_recv()
    ow_pass(last).start()
    ow_across(last - 1).wait_recv()
    ow_pass(last - 1).start()
    TOT[...] = jnp.zeros(TOT.shape, jnp.float32)

    def add_head(i, carry):
        @pl.when(i == 2 * L)
        def _():
            for j in range(last + 1):
                ow_pass(j).wait_recv()

        h = (x * 2 * L + i) % (T * L)
        remote(HO.at[0, 0], HI.at[h], h_send.at[0, 0], h_recv.at[h], s, mate).wait_recv()
        TOT[...] += jnp.dot(HI[h], W[h], preferred_element_type=jnp.float32)
        return carry

    lax.fori_loop(0, T * L, add_head, 0)
    out[...] = TOT[...].astype(jnp.bfloat16)

    act_across().wait_send()
    act_mate().wait_send()
    act_pass().wait_send()
    ow_mate().wait_send()
    for i in range(H):
        ow_beside(i, y).wait_send()
    for j in range(last):
        ow_across(j).wait_send()
    for j in range(last + 1):
        ow_pass(j).wait_send()
    lam_out().wait_send()
    for l in range(L):
        for xx in range(X):
            for d in range(2):
                @pl.when(jnp.logical_not(stays(l, d)))
                def _():
                    piece(l, xx, d).wait_send()

    def drain(zs, carry):
        for xx in range(X):
            to_beside(zs, xx).wait_send()
            to_mate(zs, xx).wait_send()
            to_mate_again(zs, xx).wait_send()

            @pl.when(jnp.logical_not(ends_here(zs, xx)))
            def _():
                home(zs, xx).wait_send()

        return carry

    lax.fori_loop(0, Z, drain, 0)


def fused(S, T, L, activations, query_weight, key_weight, value_weight, out_weight, lambdas, head_gain):
    R, D = activations.shape
    X, Y = 2, 2
    Z = S // Y
    bf, f32 = jnp.bfloat16, jnp.float32
    vmem = pl.BlockSpec(memory_space=pltpu.VMEM)
    hbm = pl.BlockSpec(memory_space=pl.ANY)
    smem = pl.BlockSpec(memory_space=pltpu.SMEM)
    dma = pltpu.SemaphoreType.DMA
    width = query_weight.shape[1]
    return pl.pallas_call(
        functools.partial(layer_kernel, S, T, L, R),
        out_shape=jax.ShapeDtypeStruct((R, D), bf),
        in_specs=[vmem, hbm, hbm, hbm, hbm, smem, vmem],
        out_specs=vmem,
        scratch_shapes=[
            pltpu.VMEM((T, R, D), bf),
            pltpu.VMEM((3, D, width), bf),
            pltpu.VMEM((T * L, VALUE, D), bf),
            pltpu.VMEM((L, X, 2, R, 768), bf),
            pltpu.VMEM((Z, X, R, 768), bf),
            pltpu.VMEM((S * T * R, 512), bf),
            pltpu.VMEM((Z, X, R, VALUE), bf),
            pltpu.VMEM((T * L, R, VALUE), bf),
            pltpu.VMEM((L, 8, 128), f32),
            pltpu.VMEM((L, 8, 128), f32),
            pltpu.VMEM((Z, 2, X * R, VALUE), f32),
            pltpu.VMEM((Z, 2, X * R, 128), f32),
            pltpu.VMEM((Z, 2, X * R, 128), f32),
            pltpu.VMEM((R, D), f32),
            dma((3,)), dma((2,)),
            dma((3,)), dma((T,)),
            dma((1,)), dma((1,)),
            dma((2 * L - 1 + Z // 2,)), dma((2 * L - 1 + Z // 2,)),
            dma((2 * L + 1,)), dma((2 * L + 1,)),
            dma((L, X, 2)), dma((Z, X)),
            dma((3, Z, X)), dma((4, Z, X)),
            dma((Z, X)), dma((T * L,)),
        ],
        compiler_params=pltpu.CompilerParams(
            has_side_effects=True, collective_id=0, vmem_limit_bytes=60 * 1024 * 1024
        ),
    )(
        activations, query_weight, key_weight, value_weight,
        out_weight.reshape(L, VALUE, D), lambdas, head_gain.reshape(1, VALUE),
    )


def empty_state(count, local_heads):
    return (
        jnp.full((local_heads, 2, count), very_low, jnp.float32),
        jnp.zeros((local_heads, 2, count), jnp.float32),
        jnp.zeros((local_heads, 2, count, VALUE), jnp.float32),
    )


def absorb(state, query_set, query_pos, key_block, value_block, key_first):
    running, denoms, accums = state
    local_heads = running.shape[0]
    span = key_block.shape[0]
    key_grid = key_block.reshape(span, local_heads, 2, HEAD)
    scores = jnp.einsum(
        "qhme,khme->hmqk", query_set, key_grid, preferred_element_type=jnp.float32
    ) * HEAD ** (-0.5)
    key_pos = key_first + jnp.arange(span, dtype=jnp.int32)
    allowed = key_pos[None, :] <= query_pos[:, None]
    masked = jnp.where(allowed, scores, very_low)
    updated = jnp.maximum(running, jnp.max(masked, axis=-1))
    exp_weights = jnp.where(allowed, jnp.exp(masked - updated[..., None]), 0.0)
    factor = jnp.exp(running - updated)
    denoms = denoms * factor + jnp.sum(exp_weights, axis=-1)
    value_grid = value_block.reshape(span, local_heads, VALUE)
    product = jnp.einsum(
        "hmqk,khv->hmqv",
        exp_weights.astype(jnp.bfloat16),
        value_grid,
        preferred_element_type=jnp.float32,
    )
    accums = accums * factor[..., None] + product
    return (updated, denoms, accums)


def make_folder(query_sets, carry, pieces):
    key_piece, value_piece = pieces
    length = key_piece.shape[0]
    span = math.gcd(length, 512)

    def one_span(span_index, states):
        offset = span_index * span
        key_block = lax.dynamic_slice_in_dim(key_piece, offset, span, 0)
        value_block = lax.dynamic_slice_in_dim(value_piece, offset, span, 0)
        fresh = []
        for state, query_entry in zip(states, query_sets):
            query_set, query_pos = query_entry

            def take(current):
                return absorb(current, query_set, query_pos, key_block, value_block, offset)

            def leave(current):
                return current

            fresh.append(lax.cond(offset <= query_pos[-1], take, leave, state))
        return tuple(fresh)

    return lax.fori_loop(0, length // span, one_span, carry)


def shards(activations, query_weight, key_weight, value_weight, out_weight, lambdas, head_gain):
    local_heads = lambdas.shape[0]
    query_width = query_weight.shape[1]
    joined_weight = jnp.concatenate([query_weight, key_weight, value_weight], axis=1)
    projected = jnp.dot(
        lax.all_gather(activations, "tp", axis=0, tiled=True),
        joined_weight,
        preferred_element_type=jnp.float32,
    ).astype(jnp.bfloat16)
    row_count = projected.shape[0]
    queries = projected[:, :query_width].reshape(row_count, local_heads, 2, HEAD)
    key_rows = projected[:, query_width : 2 * query_width]
    value_rows = projected[:, 2 * query_width :]
    position = lax.axis_index("sp") * row_count + jnp.arange(row_count, dtype=jnp.int32)
    query_sets = [(queries, position)]
    start_states = tuple((empty_state(entry[0].shape[0], local_heads) for entry in query_sets))
    finals = make_folder(
        query_sets,
        start_states,
        (
            lax.all_gather(key_rows, "sp", axis=0, tiled=True),
            lax.all_gather(value_rows, "sp", axis=0, tiled=True),
        ),
    )
    outputs = []
    for state in finals:
        running, denoms, accums = state
        combined = (
            accums[:, 0] / denoms[:, 0, :, None]
            - lambdas[:, None, None] * accums[:, 1] / denoms[:, 1, :, None]
        )
        inverse_rms = lax.rsqrt(jnp.mean(combined * combined, axis=-1, keepdims=True) + norm_floor)
        normed = (combined * inverse_rms * head_gain).astype(jnp.bfloat16)
        outputs.append(
            jnp.transpose(normed, (1, 0, 2)).reshape(normed.shape[1], local_heads * VALUE)
        )
    heads_out = outputs[0]
    return lax.psum_scatter(
        jnp.dot(heads_out, out_weight, preferred_element_type=jnp.float32).astype(jnp.bfloat16),
        "tp",
        scatter_dimension=0,
        tiled=True,
    )


def solution(mesh):
    in_specs = (
        P(("sp", "tp"), None),
        P(None, "tp"),
        P(None, "tp"),
        P(None, "tp"),
        P("tp", None),
        P("tp"),
        P(),
    )
    out_specs = P(("sp", "tp"), None)
    S, T = mesh.shape["sp"], mesh.shape["tp"]

    def layer(*args):
        L = args[5].shape[0] // T
        rows = args[0].shape[0] // (S * T)
        fits = T == 4 and L == 2 and S == L * T and rows % 16 == 0
        local = functools.partial(fused, S, T, L) if fits else shards
        return jax.shard_map(
            local, mesh=mesh, in_specs=in_specs, out_specs=out_specs, check_vma=False
        )(*args)

    return layer
```

profile of v0, /device:TPU:21, one launch (start us, length us, event | category | flops | bytes accessed | tf_op | source)
XLA Modules:
  0.0 77.5 jit_solution(1955944072952535446)
XLA Ops:
  0.0 75.7 %shard_map.73 = bf16[112,2048]{1,0:T(8,128)(2,1)} custom-call(bf16[112,2048]{1,0:T(8,128)(2,1)} %act.1, bf16[2048,512]{1,0:T(8,128)(2,1)} %qw.1, bf16[2048,512]{1,0:T(8,128)(2,1)} %kw.1, bf16[2048,512]{1,0:T(8,128)(2,1)} %vw.1, bf16[2,256,2048]{2,1,0:T(8,128)(2,1)} %bitcast.2, f32[2]{0:T(128)} %lam_in.1, f32[1,256]{1,0:T(1,128)} %bitcast.3), custom_call_target="tpu_custom_call" | custom-call | tf_op jit(solution)/shard_map/pallas_call | solution.py:414
  75.7 1.8 %copy.9 = bf16[112,2048]{1,0:T(8,128)(2,1)} copy(bf16[112,2048]{1,0:T(8,128)(2,1)} %shard_map.73) | data formatting | bytes 917504
where the time goes:
time: 77.7 us; the launch traced here: 77.5 us
  Pallas kernels  75.7 us (97%)
  local copies, waits for them, and re-layouts  1.82 us (2%)
    pallas_call x1, Pallas kernels, fused(): pl.pallas_call(functools.partial(layer_kernel, S, T, L, R), out_shape=jax...  75.7 us
    unnamed x1, local copies, waits for them, and re-layouts  1.82 us

commit v1 on v0

--- a/solution.py
+++ b/solution.py
@@ -22,7 +22,8 @@
     act, qw, kw, vw, ow, lam_in, gain,
     out,
     A, WP, W, PR, PC, KV, HO, HI, LS, LB, ACC, MX, DN, TOT,
-    w_sem, own_sem, a_send, a_recv, lam_send, lam_recv, o_send, o_recv, m_send, m_recv,
+    w_sem, own_sem, a_send, a_recv, lam_send, lam_recv,
+    ox_send, ox_recv, oy_send, oy_recv, m_send, m_recv,
     p_send, p_recv, f_send, f_recv, h_send, h_recv,
 ):
     X, Y = 2, 2
@@ -34,11 +35,17 @@
     c = t % 2
     y = s % Y
     z = s // Y
+    half = z // H
+    low = z % H
     mate = x * 2 + (1 - c)
     across = (1 - x) * 2 + c
+    diagonal = (1 - x) * 2 + (1 - c)
     beside = z * Y + (1 - y)
-    upper = z // (Z // 2)
-    near = upper * (Z // 2)
+    pair = (half * H + 1 - low) * Y + y
+    side = (low + y) % 2
+    near = half * H + 1 - low
+    outer = (1 - half) * (Z - 1)
+    inner = (1 - half) * H + half * (H - 1)
     head = x * 2 * L + z
     span = T * R
     scale = HEAD ** (-0.5) * math.log2(math.e)
@@ -49,8 +56,17 @@
             device_id=(sp, tp), device_id_type=MESH,
         )
 
-    def weight_copy(k):
-        return pltpu.make_async_copy((qw, kw, vw)[k], WP.at[k], w_sem.at[k])
+    first_head = jnp.where(c == half, 1 - low, c)
+
+    def head_at(i):
+        return first_head if i == 0 else 1 - first_head
+
+    def weight_copy(i, part):
+        l = head_at(i)
+        return pltpu.make_async_copy(
+            (qw, kw, vw)[part].at[:, pl.ds(pl.multiple_of(l * 256, 256), 256)],
+            WP.at[l, :, part * 256:(part + 1) * 256], w_sem.at[i, part],
+        )
 
     def own_act():
         return pltpu.make_async_copy(act, A.at[t], own_sem.at[0])
@@ -59,73 +75,69 @@
         return pltpu.make_async_copy(ow, W.at[pl.ds(t * L, L)], own_sem.at[1])
 
     def act_across():
-        return remote(act, A.at[t], a_send.at[0], a_recv.at[t], s, across)
+        return remote(A.at[t], A.at[t], a_send.at[0], a_recv.at[t], s, across)
 
     def act_mate():
-        return remote(act, A.at[t], a_send.at[1], a_recv.at[t], s, mate)
+        return remote(A.at[t], A.at[t], a_send.at[1], a_recv.at[t], s, mate)
 
     def act_pass():
         return remote(A.at[across], A.at[across], a_send.at[2], a_recv.at[across], s, mate)
 
     def wait_act(i):
-        remote(act, A.at[i], a_send.at[0], a_recv.at[i], s, mate).wait_recv()
-
-    def quarter(owner, q):
-        rows = pl.ds(pl.multiple_of((q % 2) * (VALUE // 2), VALUE // 2), VALUE // 2)
-        return owner * L + q // 2, rows
-
-    def turn(j, row):
-        return row * (2 * L - 1) if j == 0 else j
-
-    def ow_across(j):
-        q = turn(j, y)
-        place, rows = quarter(t, q)
+        remote(A.at[i], A.at[i], a_send.at[0], a_recv.at[i], s, mate).wait_recv()
+
+    cut = VALUE // 4
+    order = (0, 2, 3, 1)
+
+    def slab(owner, l, k):
+        return W.at[owner * L + l, pl.ds(k * cut, cut)]
+
+    def ow_across(k):
+        l, q = (side, order[k]) if k < 4 else (1 - side, 1)
         return remote(
-            ow.at[q // 2, rows], W.at[place, rows], o_send.at[j], o_recv.at[j], s, across
-        )
+            ow.at[l, pl.ds(q * cut, cut)], slab(t, l, q), ox_send.at[k], ox_recv.at[k], s, across
+        )
+
+    def ow_side(k, l):
+        part = slab(across, l, order[k])
+        target = beside if k == 0 else pair
+        return remote(part, part, oy_send.at[k], oy_recv.at[k], target, t)
+
+    def ow_pass(k):
+        l, q = (side, order[k]) if k < 4 else (1 - side, (1, 0, 2, 3)[k - 4])
+        part = slab(across, l, q)
+        return remote(part, part, m_send.at[k], m_recv.at[k], s, mate)
 
     def ow_mate():
-        return remote(ow, W.at[pl.ds(t * L, L)], m_send.at[0], m_recv.at[0], s, mate)
-
-    last = 2 * L - 1
-
-    cut = VALUE // 2 // H
-
-    def ow_beside(k, row):
-        q = turn(0, row)
-        first = pl.multiple_of((q % 2) * (VALUE // 2) + k * cut, cut)
-        part = W.at[across * L + q // 2, pl.ds(first, cut)]
-        return remote(part, part, o_send.at[last + k], o_recv.at[last + k], beside, t)
-
-    def ow_pass(j):
-        q = turn(0, 1 - y) if j == last else turn(j, y)
-        place, rows = quarter(across, q)
-        part = W.at[place, rows]
-        return remote(part, part, m_send.at[1 + j], m_recv.at[1 + j], s, mate)
+        return remote(ow, W.at[pl.ds(t * L, L)], m_send.at[8], m_recv.at[8], s, mate)
 
     def lam_out():
         return remote(LS, LB, lam_send.at[0], lam_recv.at[0], s, mate)
 
     barrier = pltpu.get_barrier_semaphore()
+    own_act().start()
+    for i in range(L):
+        for part in range(3):
+            weight_copy(i, part).start()
     greeted = [(beside, t)]
     for i in range(Z):
         row = ((z + i) % Z) * Y + y
         greeted += [(row, mate), (row, across)] + ([(row, t)] if i > 0 else [])
     for sp, tp in greeted:
         pl.semaphore_signal(barrier, inc=1, device_id=(sp, tp), device_id_type=MESH)
-    weight_copies = [weight_copy(k) for k in range(3)]
-    for copy in weight_copies:
-        copy.start()
-    own_act().start()
     own_ow().start()
-    pl.semaphore_wait(barrier, len(greeted))
-
     for l in range(L):
         LS[l] = jnp.full((8, 128), lam_in[l], jnp.float32)
+    MX[...] = jnp.full(MX.shape, very_low, jnp.float32)
+    DN[...] = jnp.zeros(DN.shape, jnp.float32)
+    ACC[...] = jnp.zeros(ACC.shape, jnp.float32)
+    own_act().wait()
+    pl.semaphore_wait(barrier, len(greeted))
+
     act_across().start()
     act_mate().start()
-    for j in range(last):
-        ow_across(j).start()
+    for k in range(5):
+        ow_across(k).start()
 
     def piece_sp(l):
         return (c * L + l) * Y + y
@@ -148,31 +160,14 @@
         def _():
             piece(l, xx, d).start()
 
-    def project(xx):
+    def project(xx, i):
+        l = head_at(i)
         rows = A[pl.ds(xx * 2, 2)].reshape(2 * R, A.shape[2])
-        for part in range(3):
-            got = jnp.dot(rows, WP[part], preferred_element_type=jnp.float32)
-            if part == 0:
-                got = got * scale
-            got = got.astype(jnp.bfloat16)
-            for l in range(L):
-                cols = got[:, l * 256:(l + 1) * 256]
-                PR[l, xx, :, :, part * 256:(part + 1) * 256] = cols.reshape(2, R, 256)
-        for i in range(L):
-            l = upper * i + (1 - upper) * (L - 1 - i)
-            for d in range(2):
-                send_piece(l, xx, d)
-
-    own_act().wait()
-    for k in range(3):
-        weight_copy(k).wait()
-    wait_act(mate)
-    project(x)
-    lam_out().start()
-    wait_act(across)
-    act_pass().start()
-    wait_act((1 - x) * 2 + (1 - c))
-    project(1 - x)
+        got = jnp.dot(rows, WP[l], preferred_element_type=jnp.float32)
+        PR[l, xx, :, :, :256] = (got[:, :256] * scale).astype(jnp.bfloat16).reshape(2, R, 256)
+        PR[l, xx, :, :, 256:] = got[:, 256:].astype(jnp.bfloat16).reshape(2, R, 512)
+        for d in range(2):
+            send_piece(l, xx, d)
 
     def kv_rows(row, zs, xx, core):
         return pl.ds(((zs * Y + row) * T + xx * 2 + core) * R, R)
@@ -201,39 +196,15 @@
             kv_part(zs, xx), KV.at[kv_rows(y, zs, xx, c)], f_recv.at[3, zs, xx]
         )
 
-    def place(i):
-        return (near + i) % Z, (x + i // Z) % X
-
-    def forward(i):
-        zs, xx = place(i)
+    def forward(zs, xx):
         remote(PR.at[0, 0, 0], PC.at[zs, xx], p_send.at[0, 0, 0], p_recv.at[zs, xx], s, mate).wait_recv()
         to_beside(zs, xx).start()
         to_mate(zs, xx).start()
         to_self(zs, xx).start()
 
-    def relay(i):
-        zs, xx = place(i)
+    def relay(zs, xx):
         to_beside(zs, xx).wait_recv()
         to_mate_again(zs, xx).start()
-
-    def spread(first, count, weights):
-        def both(i, carry):
-            forward(first + i)
-            if weights:
-                @pl.when(i == 0)
-                def _():
-                    ow_across(0).wait_recv()
-
-                ow_beside(i, y).start()
-
-            @pl.when(i > 0)
-            def _():
-                relay(first + i - 1)
-
-            return carry
-
-        lax.fori_loop(0, count, both, 0)
-        relay(first + count - 1)
 
     def wait_plane(zs):
         for xx in range(X):
@@ -244,39 +215,28 @@
     q_rows = X * R
     k_rows = Y * span
 
-    def chunk(i, j, masked):
+    def chunk(i, j):
+        row = lax.broadcasted_iota(jnp.int32, (q_rows, 1), 0)
+        col = lax.broadcasted_iota(jnp.int32, (q_rows, k_rows), 1)
+        pos = row + jnp.where(row >= R, R, 0) + (y * span + c * R + (i - j) * k_rows)
+        seen = col <= pos
+        values = KV[pl.ds(j * k_rows, k_rows), 256:512]
         for m in range(2):
             q = PC[i, :, :, m * 128:(m + 1) * 128].reshape(q_rows, 128)
             keys = KV[pl.ds(j * k_rows, k_rows), m * 128:(m + 1) * 128]
             sc = lax.dot_general(
                 q, keys, (((1,), (1,)), ((), ())), preferred_element_type=jnp.float32
             )
-            if masked:
-                row = lax.broadcasted_iota(jnp.int32, (q_rows, 1), 0)
-                col = lax.broadcasted_iota(jnp.int32, (q_rows, k_rows), 1)
-                pos = row + jnp.where(row >= R, R, 0) + (y * span + c * R)
-                sc = jnp.where(col <= pos, sc, very_low)
+            sc = jnp.where(seen, sc, very_low)
             old = MX[i, m, :, :1]
             new = jnp.maximum(old, jnp.max(sc, axis=1, keepdims=True))
             p = jnp.exp2(sc - new)
             factor = jnp.exp2(old - new)
             total = DN[i, m, :, :1] * factor + jnp.sum(p, axis=1, keepdims=True)
-            values = KV[pl.ds(j * k_rows, k_rows), 256:512]
             got = jnp.dot(p.astype(jnp.bfloat16), values, preferred_element_type=jnp.float32)
             ACC[i, m] = ACC[i, m] * factor + got
             MX[i, m] = jnp.broadcast_to(new, MX.shape[2:])
             DN[i, m] = jnp.broadcast_to(total, DN.shape[2:])
-
-    def chunks(i, low, high, diagonal):
-        def inner(j, carry):
-            chunk(i, j, False)
-            return carry
-
-        lax.fori_loop(low, high, inner, 0)
-
-        @pl.when(diagonal)
-        def _():
-            chunk(i, i, True)
 
     def home(zs, xx):
         return remote(
@@ -303,64 +263,120 @@
             def _():
                 home(i, xx).start()
 
-    MX[...] = jnp.full(MX.shape, very_low, jnp.float32)
-    DN[...] = jnp.zeros(DN.shape, jnp.float32)
-    ACC[...] = jnp.zeros(ACC.shape, jnp.float32)
-    spread(0, Z + H, False)
+    for part in range(3):
+        weight_copy(0, part).wait()
+    wait_act(mate)
+    project(x, 0)
+    for part in range(3):
+        weight_copy(1, part).wait()
+    project(x, 1)
+    lam_out().start()
+    ow_mate().start()
+    forward(z, x)
+    relay(z, x)
+    wait_act(across)
+    act_pass().start()
+    wait_act(diagonal)
+    project(1 - x, 0)
+    forward(near, x)
+    project(1 - x, 1)
+    forward(z, 1 - x)
+    forward(outer, x)
+    relay(near, x)
+    relay(z, 1 - x)
+    ow_across(0).wait_recv()
+    ow_side(0, side).start()
+    ow_pass(0).start()
+    forward(near, 1 - x)
+    relay(outer, x)
+    forward(inner, x)
+    relay(near, 1 - x)
+    ow_across(1).wait_recv()
+    ow_side(1, side).start()
+    ow_pass(1).start()
     lam_out().wait_recv()
-    for i in range(H):
-        wait_plane(near + i)
-
-    def step(k, carry):
-        @pl.when(k == H)
-        def _():
-            spread(Z + H, H, True)
-            ow_mate().start()
-            for i in range(H):
-                wait_plane((near + H + i) % Z)
-
-        @pl.when(k == Z - 1)
-        def _():
-            ow_pass(0).start()
-            for j in range(1, last - 1):
-                ow_across(j).wait_recv()
-                ow_pass(j).start()
-
-        early = k < H
-        i = jnp.where(early, near + k, jnp.where(upper == 1, k - H, Z - 1 - (k - H)))
-        partial = (upper == 1) & (i >= H)
-        low = jnp.where(early, near, 0)
-        high = jnp.where(partial & jnp.logical_not(early), H, i)
-        used = (upper == 1) | (k < Z)
-
-        @pl.when(used)
-        def _():
-            chunks(i, low, high, jnp.logical_not(partial) | early)
-
-            @pl.when(jnp.logical_not(partial & early))
-            def _():
-                finish(i)
+    wait_plane(z)
+    wait_plane(near)
+
+    def near_step(k, carry):
+        @pl.when(k == 1)
+        def _():
+            relay(inner, x)
+            ow_side(0, 1 - side).wait_recv()
+            ow_pass(5).start()
+
+        i = half * H + jnp.where(k == 0, 0, 1)
+        chunk(i, half * H + k // 2)
+
+        @pl.when((half == 0) & (k != 1))
+        def _():
+            finish(i)
 
         return carry
 
-    lax.fori_loop(0, Z + H, step, 0)
+    lax.fori_loop(0, 3, near_step, 0)
+    forward(outer, 1 - x)
+    ow_across(2).wait_recv()
+    ow_side(2, side).start()
+    ow_pass(2).start()
+    relay(outer, 1 - x)
+    wait_plane(outer)
+
+    def outer_step(k, carry):
+        @pl.when(k == 2)
+        def _():
+            forward(inner, 1 - x)
+
+        i = jnp.where(half == 0, Z - 1, jnp.where(k == 0, 0, k + 1))
+        j = jnp.where(half == 0, jnp.where(k == 0, Z - 1, k - 1), 0)
+        chunk(i, j)
+
+        @pl.when((half == 1) & (k == 0))
+        def _():
+            finish(i)
+
+        return carry
+
+    lax.fori_loop(0, 3, outer_step, 0)
+    ow_across(3).wait_recv()
+    ow_pass(3).start()
+    relay(inner, 1 - x)
+    ow_side(1, 1 - side).wait_recv()
+    ow_pass(6).start()
+    wait_plane(inner)
+
+    def inner_step(k, carry):
+        @pl.when(k == 3)
+        def _():
+            ow_across(4).wait_recv()
+            ow_pass(4).start()
+
+        i = jnp.where(k < 2, inner, jnp.where((half == 0) & (k == 2), inner, k))
+        j = jnp.where(k == 0, inner, jnp.where(k == 1, 0, jnp.where((half == 0) & (k == 3), inner, 1)))
+        chunk(i, j)
+
+        @pl.when((half == 1) & (k > 0) | (k > 1))
+        def _():
+            finish(i)
+
+        return carry
+
+    lax.fori_loop(0, 4, inner_step, 0)
 
     own_ow().wait()
     ow_mate().wait_recv()
-    for i in range(H):
-        ow_beside(i, 1 - y).wait_recv()
-    ow_pass(last).start()
-    ow_across(last - 1).wait_recv()
-    ow_pass(last - 1).start()
+    ow_side(2, 1 - side).wait_recv()
+    ow_pass(7).start()
     TOT[...] = jnp.zeros(TOT.shape, jnp.float32)
 
     def add_head(i, carry):
-        @pl.when(i == 2 * L)
-        def _():
-            for j in range(last + 1):
-                ow_pass(j).wait_recv()
-
-        h = (x * 2 * L + i) % (T * L)
+        @pl.when(i == 2)
+        def _():
+            for k in range(8):
+                ow_pass(k).wait_recv()
+
+        plane = (half * H + i // 4 * H + i % 2) % Z
+        h = ((x + i // 2) % 2) * 2 * L + plane
         remote(HO.at[0, 0], HI.at[h], h_send.at[0, 0], h_recv.at[h], s, mate).wait_recv()
         TOT[...] += jnp.dot(HI[h], W[h], preferred_element_type=jnp.float32)
         return carry
@@ -372,12 +388,12 @@
     act_mate().wait_send()
     act_pass().wait_send()
     ow_mate().wait_send()
-    for i in range(H):
-        ow_beside(i, y).wait_send()
-    for j in range(last):
-        ow_across(j).wait_send()
-    for j in range(last + 1):
-        ow_pass(j).wait_send()
+    for k in range(5):
+        ow_across(k).wait_send()
+    for k in range(3):
+        ow_side(k, side).wait_send()
+    for k in range(8):
+        ow_pass(k).wait_send()
     lam_out().wait_send()
     for l in range(L):
         for xx in range(X):
@@ -414,11 +430,11 @@
     return pl.pallas_call(
         functools.partial(layer_kernel, S, T, L, R),
         out_shape=jax.ShapeDtypeStruct((R, D), bf),
-        in_specs=[vmem, hbm, hbm, hbm, hbm, smem, vmem],
+        in_specs=[hbm, hbm, hbm, hbm, hbm, smem, vmem],
         out_specs=vmem,
         scratch_shapes=[
             pltpu.VMEM((T, R, D), bf),
-            pltpu.VMEM((3, D, width), bf),
+            pltpu.VMEM((L, D, 3 * width // L), bf),
             pltpu.VMEM((T * L, VALUE, D), bf),
             pltpu.VMEM((L, X, 2, R, 768), bf),
             pltpu.VMEM((Z, X, R, 768), bf),
@@ -431,11 +447,10 @@
             pltpu.VMEM((Z, 2, X * R, 128), f32),
             pltpu.VMEM((Z, 2, X * R, 128), f32),
             pltpu.VMEM((R, D), f32),
-            dma((3,)), dma((2,)),
+            dma((L, 3)), dma((2,)),
             dma((3,)), dma((T,)),
             dma((1,)), dma((1,)),
-            dma((2 * L - 1 + Z // 2,)), dma((2 * L - 1 + Z // 2,)),
-            dma((2 * L + 1,)), dma((2 * L + 1,)),
+            dma((5,)), dma((5,)), dma((3,)), dma((3,)), dma((9,)), dma((9,)),
             dma((L, X, 2)), dma((Z, X)),
             dma((3, Z, X)), dma((4, Z, X)),
             dma((Z, X)), dma((T * L,)),

time: 77.7 us -> 73.2 us (0.942)
  the two profiles are of different devices: /device:TPU:21 before, /device:TPU:24 now
where the time goes in v1:
time: 73.2 us; the launch traced here: 73 us
  Pallas kernels  71.2 us (97%)
  local copies, waits for them, and re-layouts  1.82 us (2%)
    pallas_call x1, Pallas kernels, fused(): pl.pallas_call(functools.partial(layer_kernel, S, T, L, R), out_shape=jax...  71.2 us
    unnamed x1, local copies, waits for them, and re-layouts  1.82 us

profile of v1, /device:TPU:24, one launch (start us, length us, event | category | flops | bytes accessed | tf_op | source)
XLA Modules:
  0.0 73.0 jit_solution(2572219204645589219)
XLA Ops:
  0.0 71.2 %shard_map.73 = bf16[112,2048]{1,0:T(8,128)(2,1)} custom-call(bf16[112,2048]{1,0:T(8,128)(2,1)} %act.1, bf16[2048,512]{1,0:T(8,128)(2,1)} %qw.1, bf16[2048,512]{1,0:T(8,128)(2,1)} %kw.1, bf16[2048,512]{1,0:T(8,128)(2,1)} %vw.1, bf16[2,256,2048]{2,1,0:T(8,128)(2,1)} %bitcast.2, f32[2]{0:T(128)} %lam_in.1, f32[1,256]{1,0:T(1,128)} %bitcast.3), custom_call_target="tpu_custom_call" | custom-call | tf_op jit(solution)/shard_map/pallas_call | solution.py:430
  71.2 1.8 %copy.9 = bf16[112,2048]{1,0:T(8,128)(2,1)} copy(bf16[112,2048]{1,0:T(8,128)(2,1)} %shard_map.73) | data formatting | bytes 917504

commit v2 on v1

--- a/solution.py
+++ b/solution.py
@@ -44,8 +44,12 @@
     pair = (half * H + 1 - low) * Y + y
     side = (low + y) % 2
     near = half * H + 1 - low
-    outer = (1 - half) * (Z - 1)
-    inner = (1 - half) * H + half * (H - 1)
+    third = (1 - half) * H
+    last = third + 1
+    edge = (z == 0) | (z == Z - 1)
+    early = jnp.where(edge, third, near)
+    later = jnp.where(edge, near, third)
+    held = (z == Z - 1) & (c != half)
     head = x * 2 * L + z
     span = T * R
     scale = HEAD ** (-0.5) * math.log2(math.e)
@@ -116,22 +120,19 @@
 
     barrier = pltpu.get_barrier_semaphore()
     own_act().start()
-    for i in range(L):
-        for part in range(3):
-            weight_copy(i, part).start()
     greeted = [(beside, t)]
     for i in range(Z):
         row = ((z + i) % Z) * Y + y
         greeted += [(row, mate), (row, across)] + ([(row, t)] if i > 0 else [])
     for sp, tp in greeted:
         pl.semaphore_signal(barrier, inc=1, device_id=(sp, tp), device_id_type=MESH)
-    own_ow().start()
     for l in range(L):
         LS[l] = jnp.full((8, 128), lam_in[l], jnp.float32)
-    MX[...] = jnp.full(MX.shape, very_low, jnp.float32)
-    DN[...] = jnp.zeros(DN.shape, jnp.float32)
-    ACC[...] = jnp.zeros(ACC.shape, jnp.float32)
     own_act().wait()
+    for i in range(L):
+        for part in range(3):
+            weight_copy(i, part).start()
+    own_ow().start()
     pl.semaphore_wait(barrier, len(greeted))
 
     act_across().start()
@@ -166,8 +167,18 @@
         got = jnp.dot(rows, WP[l], preferred_element_type=jnp.float32)
         PR[l, xx, :, :, :256] = (got[:, :256] * scale).astype(jnp.bfloat16).reshape(2, R, 256)
         PR[l, xx, :, :, 256:] = got[:, 256:].astype(jnp.bfloat16).reshape(2, R, 512)
-        for d in range(2):
-            send_piece(l, xx, d)
+
+        @pl.when(jnp.logical_not(held))
+        def _():
+            for d in range(2):
+                send_piece(l, xx, d)
+
+    def send_held(xx):
+        @pl.when(held)
+        def _():
+            for i in range(L):
+                for d in range(2):
+                    piece(head_at(i), xx, d).start()
 
     def kv_rows(row, zs, xx, core):
         return pl.ds(((zs * Y + row) * T + xx * 2 + core) * R, R)
@@ -270,41 +281,42 @@
     for part in range(3):
         weight_copy(1, part).wait()
     project(x, 1)
+    forward(z, x)
     lam_out().start()
     ow_mate().start()
-    forward(z, x)
+    MX[...] = jnp.full(MX.shape, very_low, jnp.float32)
+    DN[...] = jnp.zeros(DN.shape, jnp.float32)
+    ACC[...] = jnp.zeros(ACC.shape, jnp.float32)
+    forward(early, x)
+    send_held(x)
     relay(z, x)
     wait_act(across)
     act_pass().start()
+    forward(later, x)
     wait_act(diagonal)
     project(1 - x, 0)
-    forward(near, x)
     project(1 - x, 1)
     forward(z, 1 - x)
-    forward(outer, x)
-    relay(near, x)
+    relay(early, x)
+    relay(later, x)
+    forward(last, x)
+    forward(near, 1 - x)
     relay(z, 1 - x)
+    send_held(1 - x)
+    forward(third, 1 - x)
     ow_across(0).wait_recv()
     ow_side(0, side).start()
     ow_pass(0).start()
-    forward(near, 1 - x)
-    relay(outer, x)
-    forward(inner, x)
-    relay(near, 1 - x)
     ow_across(1).wait_recv()
     ow_side(1, side).start()
     ow_pass(1).start()
+    relay(last, x)
+    relay(near, 1 - x)
     lam_out().wait_recv()
     wait_plane(z)
     wait_plane(near)
 
     def near_step(k, carry):
-        @pl.when(k == 1)
-        def _():
-            relay(inner, x)
-            ow_side(0, 1 - side).wait_recv()
-            ow_pass(5).start()
-
         i = half * H + jnp.where(k == 0, 0, 1)
         chunk(i, half * H + k // 2)
 
@@ -315,75 +327,57 @@
         return carry
 
     lax.fori_loop(0, 3, near_step, 0)
-    forward(outer, 1 - x)
+    relay(third, 1 - x)
     ow_across(2).wait_recv()
     ow_side(2, side).start()
     ow_pass(2).start()
-    relay(outer, 1 - x)
-    wait_plane(outer)
-
-    def outer_step(k, carry):
-        @pl.when(k == 2)
-        def _():
-            forward(inner, 1 - x)
-
-        i = jnp.where(half == 0, Z - 1, jnp.where(k == 0, 0, k + 1))
-        j = jnp.where(half == 0, jnp.where(k == 0, Z - 1, k - 1), 0)
-        chunk(i, j)
-
-        @pl.when((half == 1) & (k == 0))
+    wait_plane(third)
+
+    def third_step(k, carry):
+        i = jnp.where(half == 0, H, jnp.where(k == 0, 0, k + 1))
+        chunk(i, jnp.where(half == 0, k, 0))
+
+        @pl.when(k == 0)
+        def _():
+            forward(last, 1 - x)
+
+        @pl.when(jnp.where(half == 0, k == 2, k == 0))
         def _():
             finish(i)
 
         return carry
 
-    lax.fori_loop(0, 3, outer_step, 0)
+    lax.fori_loop(0, 3, third_step, 0)
+
+    def last_step(k, carry):
+        @pl.when(k == 1)
+        def _():
+            relay(last, 1 - x)
+
+        @pl.when(k == jnp.where(half == 0, 3, 1))
+        def _():
+            wait_plane(last)
+
+        i = jnp.where(half == 0, last, jnp.where(k == 0, last, k))
+        chunk(i, jnp.where(half == 0, k, jnp.where(k == 0, 0, last)))
+
+        @pl.when(jnp.where(half == 0, k == 3, k > 0))
+        def _():
+            finish(i)
+
+        return carry
+
+    lax.fori_loop(0, 4, last_step, 0)
     ow_across(3).wait_recv()
     ow_pass(3).start()
-    relay(inner, 1 - x)
+    ow_side(0, 1 - side).wait_recv()
+    ow_pass(5).start()
     ow_side(1, 1 - side).wait_recv()
     ow_pass(6).start()
-    wait_plane(inner)
-
-    def inner_step(k, carry):
-        @pl.when(k == 3)
-        def _():
-            ow_across(4).wait_recv()
-            ow_pass(4).start()
-
-        i = jnp.where(k < 2, inner, jnp.where((half == 0) & (k == 2), inner, k))
-        j = jnp.where(k == 0, inner, jnp.where(k == 1, 0, jnp.where((half == 0) & (k == 3), inner, 1)))
-        chunk(i, j)
-
-        @pl.when((half == 1) & (k > 0) | (k > 1))
-        def _():
-            finish(i)
-
-        return carry
-
-    lax.fori_loop(0, 4, inner_step, 0)
-
-    own_ow().wait()
-    ow_mate().wait_recv()
+    ow_across(4).wait_recv()
+    ow_pass(4).start()
     ow_side(2, 1 - side).wait_recv()
     ow_pass(7).start()
-    TOT[...] = jnp.zeros(TOT.shape, jnp.float32)
-
-    def add_head(i, carry):
-        @pl.when(i == 2)
-        def _():
-            for k in range(8):
-                ow_pass(k).wait_recv()
-
-        plane = (half * H + i // 4 * H + i % 2) % Z
-        h = ((x + i // 2) % 2) * 2 * L + plane
-        remote(HO.at[0, 0], HI.at[h], h_send.at[0, 0], h_recv.at[h], s, mate).wait_recv()
-        TOT[...] += jnp.dot(HI[h], W[h], preferred_element_type=jnp.float32)
-        return carry
-
-    lax.fori_loop(0, T * L, add_head, 0)
-    out[...] = TOT[...].astype(jnp.bfloat16)
-
     act_across().wait_send()
     act_mate().wait_send()
     act_pass().wait_send()
@@ -392,8 +386,6 @@
         ow_across(k).wait_send()
     for k in range(3):
         ow_side(k, side).wait_send()
-    for k in range(8):
-        ow_pass(k).wait_send()
     lam_out().wait_send()
     for l in range(L):
         for xx in range(X):
@@ -402,12 +394,39 @@
                 def _():
                     piece(l, xx, d).wait_send()
 
-    def drain(zs, carry):
+    def settle(zs, carry):
         for xx in range(X):
             to_beside(zs, xx).wait_send()
             to_mate(zs, xx).wait_send()
             to_mate_again(zs, xx).wait_send()
 
+        return carry
+
+    lax.fori_loop(0, Z, settle, 0)
+    own_ow().wait()
+    ow_mate().wait_recv()
+    TOT[...] = jnp.zeros(TOT.shape, jnp.float32)
+
+    def add_head(i, carry):
+        @pl.when(i == 2)
+        def _():
+            for k in range(8):
+                ow_pass(k).wait_recv()
+
+        plane = (half * H + i // 4 * H + i % 2) % Z
+        h = ((x + i // 2) % 2) * 2 * L + plane
+        remote(HO.at[0, 0], HI.at[h], h_send.at[0, 0], h_recv.at[h], s, mate).wait_recv()
+        TOT[...] += jnp.dot(HI[h], W[h], preferred_element_type=jnp.float32)
+        return carry
+
+    lax.fori_loop(0, T * L, add_head, 0)
+    for k in range(8):
+        ow_pass(k).wait_send()
+    out[...] = TOT[...].astype(jnp.bfloat16)
+
+
+    def drain(zs, carry):
+        for xx in range(X):
             @pl.when(jnp.logical_not(ends_here(zs, xx)))
             def _():
                 home(zs, xx).wait_send()

time: 73.2 us -> 64.6 us (0.88)
  the two profiles are of different devices: /device:TPU:24 before, /device:TPU:25 now
where the time goes in v2:
time: 64.6 us; the launch traced here: 64.4 us
  Pallas kernels  62.6 us (97%)
  local copies, waits for them, and re-layouts  1.82 us (3%)
    pallas_call x1, Pallas kernels, fused(): pl.pallas_call(functools.partial(layer_kernel, S, T, L, R), out_shape=jax...  62.6 us
    unnamed x1, local copies, waits for them, and re-layouts  1.82 us

profile of v2, /device:TPU:25, one launch (start us, length us, event | category | flops | bytes accessed | tf_op | source)
XLA Modules:
  0.0 64.4 jit_solution(1815955290301522475)
XLA Ops:
  0.0 62.6 %shard_map.73 = bf16[112,2048]{1,0:T(8,128)(2,1)} custom-call(bf16[112,2048]{1,0:T(8,128)(2,1)} %act.1, bf16[2048,512]{1,0:T(8,128)(2,1)} %qw.1, bf16[2048,512]{1,0:T(8,128)(2,1)} %kw.1, bf16[2048,512]{1,0:T(8,128)(2,1)} %vw.1, bf16[2,256,2048]{2,1,0:T(8,128)(2,1)} %bitcast.2, f32[2]{0:T(128)} %lam_in.1, f32[1,256]{1,0:T(1,128)} %bitcast.3), custom_call_target="tpu_custom_call" | custom-call | tf_op jit(solution)/shard_map/pallas_call | solution.py:449
  62.6 1.8 %copy.9 = bf16[112,2048]{1,0:T(8,128)(2,1)} copy(bf16[112,2048]{1,0:T(8,128)(2,1)} %shard_map.73) | data formatting | bytes 917504

commit v3 on v2

--- a/solution.py
+++ b/solution.py
@@ -47,8 +47,10 @@
     third = (1 - half) * H
     last = third + 1
     edge = (z == 0) | (z == Z - 1)
-    early = jnp.where(edge, third, near)
-    later = jnp.where(edge, near, third)
+    ahead = (1 - half) * (Z - 1)
+    behind = (1 - half) * H + half * (H - 1)
+    early = jnp.where(edge, ahead, near)
+    later = jnp.where(edge, near, ahead)
     held = (z == Z - 1) & (c != half)
     head = x * 2 * L + z
     span = T * R
@@ -104,7 +106,7 @@
 
     def ow_side(k, l):
         part = slab(across, l, order[k])
-        target = beside if k == 0 else pair
+        target = beside if k == 2 else pair
         return remote(part, part, oy_send.at[k], oy_recv.at[k], target, t)
 
     def ow_pass(k):
@@ -120,6 +122,8 @@
 
     barrier = pltpu.get_barrier_semaphore()
     own_act().start()
+    for part in range(3):
+        weight_copy(0, part).start()
     greeted = [(beside, t)]
     for i in range(Z):
         row = ((z + i) % Z) * Y + y
@@ -129,9 +133,8 @@
     for l in range(L):
         LS[l] = jnp.full((8, 128), lam_in[l], jnp.float32)
     own_act().wait()
-    for i in range(L):
-        for part in range(3):
-            weight_copy(i, part).start()
+    for part in range(3):
+        weight_copy(1, part).start()
     own_ow().start()
     pl.semaphore_wait(barrier, len(greeted))
 
@@ -168,17 +171,9 @@
         PR[l, xx, :, :, :256] = (got[:, :256] * scale).astype(jnp.bfloat16).reshape(2, R, 256)
         PR[l, xx, :, :, 256:] = got[:, 256:].astype(jnp.bfloat16).reshape(2, R, 512)
 
-        @pl.when(jnp.logical_not(held))
-        def _():
-            for d in range(2):
-                send_piece(l, xx, d)
-
-    def send_held(xx):
-        @pl.when(held)
-        def _():
-            for i in range(L):
-                for d in range(2):
-                    piece(head_at(i), xx, d).start()
+    def send(xx, i):
+        for d in range(2):
+            send_piece(head_at(i), xx, d)
 
     def kv_rows(row, zs, xx, core):
         return pl.ds(((zs * Y + row) * T + xx * 2 + core) * R, R)
@@ -227,27 +222,29 @@
     k_rows = Y * span
 
     def chunk(i, j):
-        row = lax.broadcasted_iota(jnp.int32, (q_rows, 1), 0)
-        col = lax.broadcasted_iota(jnp.int32, (q_rows, k_rows), 1)
-        pos = row + jnp.where(row >= R, R, 0) + (y * span + c * R + (i - j) * k_rows)
-        seen = col <= pos
-        values = KV[pl.ds(j * k_rows, k_rows), 256:512]
+        row = lax.broadcasted_iota(jnp.int32, (q_rows, 128), 0)
+        lane = lax.broadcasted_iota(jnp.int32, (q_rows, 128), 1)
+        ahead_by = row + jnp.where(row >= R, R, 0) - lane + (y * span + c * R + (i - j) * k_rows)
+        cols = range(0, k_rows, 128)
         for m in range(2):
             q = PC[i, :, :, m * 128:(m + 1) * 128].reshape(q_rows, 128)
             keys = KV[pl.ds(j * k_rows, k_rows), m * 128:(m + 1) * 128]
             sc = lax.dot_general(
                 q, keys, (((1,), (1,)), ((), ())), preferred_element_type=jnp.float32
             )
-            sc = jnp.where(seen, sc, very_low)
-            old = MX[i, m, :, :1]
-            new = jnp.maximum(old, jnp.max(sc, axis=1, keepdims=True))
-            p = jnp.exp2(sc - new)
+            parts = [jnp.where(ahead_by >= b, sc[:, b:b + 128], very_low) for b in cols]
+            top_part = functools.reduce(jnp.maximum, parts)
+            old = MX[i, m]
+            new = jnp.maximum(old, jnp.max(top_part, axis=1, keepdims=True))
+            parts = [jnp.exp2(part - new) for part in parts]
             factor = jnp.exp2(old - new)
-            total = DN[i, m, :, :1] * factor + jnp.sum(p, axis=1, keepdims=True)
-            got = jnp.dot(p.astype(jnp.bfloat16), values, preferred_element_type=jnp.float32)
-            ACC[i, m] = ACC[i, m] * factor + got
-            MX[i, m] = jnp.broadcast_to(new, MX.shape[2:])
-            DN[i, m] = jnp.broadcast_to(total, DN.shape[2:])
+            DN[i, m] = DN[i, m] * factor + functools.reduce(jnp.add, parts)
+            MX[i, m] = new
+            p = jnp.concatenate([part.astype(jnp.bfloat16) for part in parts], axis=1)
+            values = KV[pl.ds(j * k_rows, k_rows), 256:512]
+            got = jnp.dot(p, values, preferred_element_type=jnp.float32)
+            for b in range(0, VALUE, 128):
+                ACC[i, m, :, b:b + 128] = ACC[i, m, :, b:b + 128] * factor + got[:, b:b + 128]
 
     def home(zs, xx):
         return remote(
@@ -260,7 +257,8 @@
 
     def finish(i):
         mine = jnp.where(z // L == c, LS[z % L], LB[z % L])[:1, :1]
-        comb = ACC[i, 0] / DN[i, 0, :, :1] - mine * (ACC[i, 1] / DN[i, 1, :, :1])
+        dens = [jnp.sum(DN[i, m], axis=1, keepdims=True) for m in range(2)]
+        comb = ACC[i, 0] * (1.0 / dens[0]) - ACC[i, 1] * (mine / dens[1])
         inv = lax.rsqrt(jnp.mean(comb * comb, axis=1, keepdims=True) + norm_floor)
         HO[i] = (comb * inv * gain[...]).astype(jnp.bfloat16).reshape(X, R, VALUE)
         for k in range(X):
@@ -278,9 +276,11 @@
         weight_copy(0, part).wait()
     wait_act(mate)
     project(x, 0)
+    send(x, 0)
     for part in range(3):
         weight_copy(1, part).wait()
     project(x, 1)
+    send(x, 1)
     forward(z, x)
     lam_out().start()
     ow_mate().start()
@@ -288,80 +288,93 @@
     DN[...] = jnp.zeros(DN.shape, jnp.float32)
     ACC[...] = jnp.zeros(ACC.shape, jnp.float32)
     forward(early, x)
-    send_held(x)
     relay(z, x)
     wait_act(across)
     act_pass().start()
     forward(later, x)
     wait_act(diagonal)
-    project(1 - x, 0)
-    project(1 - x, 1)
+    for i in range(L):
+        project(1 - x, i)
+
+        @pl.when(jnp.logical_not(held))
+        def _():
+            send(1 - x, i)
+
     forward(z, 1 - x)
     relay(early, x)
     relay(later, x)
-    forward(last, x)
-    forward(near, 1 - x)
+    forward(behind, x)
+    top = z == Z - 1
+    sooner = jnp.where(top, third, near)
+    after = jnp.where(top, near, third)
+    forward(sooner, 1 - x)
+
+    @pl.when(held)
+    def _():
+        for i in range(L):
+            send(1 - x, i)
+
     relay(z, 1 - x)
-    send_held(1 - x)
-    forward(third, 1 - x)
+    forward(after, 1 - x)
+    relay(behind, x)
+    relay(sooner, 1 - x)
     ow_across(0).wait_recv()
     ow_side(0, side).start()
     ow_pass(0).start()
     ow_across(1).wait_recv()
     ow_side(1, side).start()
     ow_pass(1).start()
-    relay(last, x)
-    relay(near, 1 - x)
     lam_out().wait_recv()
     wait_plane(z)
-    wait_plane(near)
-
-    def near_step(k, carry):
-        i = half * H + jnp.where(k == 0, 0, 1)
-        chunk(i, half * H + k // 2)
-
-        @pl.when((half == 0) & (k != 1))
+    wait_plane(sooner)
+
+    def body_step(k, carry):
+        upper = half == 1
+
+        @pl.when(k == 4 - half)
+        def _():
+            forward(last, 1 - x)
+
+        @pl.when(k == 3)
+        def _():
+            relay(after, 1 - x)
+            ow_across(2).wait_recv()
+            ow_pass(2).start()
+            wait_plane(after)
+
+        @pl.when(k == 5 - half)
+        def _():
+            ow_side(2, side).start()
+
+        n = k % 3
+        local = (k < 3) != top
+        i_near = half * H + jnp.where(n == 0, 0, 1)
+        i_third = jnp.where(upper, jnp.where(n == 0, 0, n + 1), H)
+        i = jnp.where(local, i_near, i_third)
+        j = jnp.where(local, half * H + n // 2, jnp.where(upper, 0, n))
+        chunk(i, j)
+
+        @pl.when(jnp.where(upper, jnp.logical_not(local) & (n == 0), jnp.where(local, n != 1, n == 2)))
         def _():
             finish(i)
 
         return carry
 
-    lax.fori_loop(0, 3, near_step, 0)
-    relay(third, 1 - x)
-    ow_across(2).wait_recv()
-    ow_side(2, side).start()
-    ow_pass(2).start()
-    wait_plane(third)
-
-    def third_step(k, carry):
-        i = jnp.where(half == 0, H, jnp.where(k == 0, 0, k + 1))
-        chunk(i, jnp.where(half == 0, k, 0))
-
-        @pl.when(k == 0)
-        def _():
-            forward(last, 1 - x)
-
-        @pl.when(jnp.where(half == 0, k == 2, k == 0))
-        def _():
-            finish(i)
-
-        return carry
-
-    lax.fori_loop(0, 3, third_step, 0)
+    lax.fori_loop(0, 6, body_step, 0)
 
     def last_step(k, carry):
-        @pl.when(k == 1)
+        @pl.when(k == 1 - half)
         def _():
             relay(last, 1 - x)
 
-        @pl.when(k == jnp.where(half == 0, 3, 1))
+        @pl.when(k == 3 * (1 - half))
         def _():
             wait_plane(last)
 
-        i = jnp.where(half == 0, last, jnp.where(k == 0, last, k))
-        chunk(i, jnp.where(half == 0, k, jnp.where(k == 0, 0, last)))
-
-        @pl.when(jnp.where(half == 0, k == 3, k > 0))
+        i = jnp.where((half == 0) | (k == 1) | (k == 2), last, jnp.where(k == 0, near, z))
+        chunk(i, jnp.where(half == 0, k, jnp.where(k == 1, 0, last)))
+
+        @pl.when(jnp.where(half == 0, k == 3, k != 1))
         def _():
             finish(i)
 
@@ -372,20 +385,10 @@
     ow_pass(3).start()
     ow_side(0, 1 - side).wait_recv()
     ow_pass(5).start()
-    ow_side(1, 1 - side).wait_recv()
-    ow_pass(6).start()
-    ow_across(4).wait_recv()
-    ow_pass(4).start()
-    ow_side(2, 1 - side).wait_recv()
-    ow_pass(7).start()
     act_across().wait_send()
     act_mate().wait_send()
     act_pass().wait_send()
     ow_mate().wait_send()
-    for k in range(5):
-        ow_across(k).wait_send()
-    for k in range(3):
-        ow_side(k, side).wait_send()
     lam_out().wait_send()
     for l in range(L):
         for xx in range(X):
@@ -410,16 +413,27 @@
     def add_head(i, carry):
         @pl.when(i == 2)
         def _():
+            ow_side(1, 1 - side).wait_recv()
+            ow_pass(6).start()
+            ow_across(4).wait_recv()
+            ow_pass(4).start()
+            ow_side(2, 1 - side).wait_recv()
+            ow_pass(7).start()
             for k in range(8):
                 ow_pass(k).wait_recv()
 
-        plane = (half * H + i // 4 * H + i % 2) % Z
-        h = ((x + i // 2) % 2) * 2 * L + plane
+        tail = i // 4
+        plane = (1 - tail) * (i % 2) + tail * (Z - 1 - (i - 4) // 2)
+        h = ((x + (1 - tail) * (i // 2) + tail * i) % 2) * 2 * L + plane
         remote(HO.at[0, 0], HI.at[h], h_send.at[0, 0], h_recv.at[h], s, mate).wait_recv()
         TOT[...] += jnp.dot(HI[h], W[h], preferred_element_type=jnp.float32)
         return carry
 
     lax.fori_loop(0, T * L, add_head, 0)
+    for k in range(5):
+        ow_across(k).wait_send()
+    for k in range(3):
+        ow_side(k, side).wait_send()
     for k in range(8):
         ow_pass(k).wait_send()
     out[...] = TOT[...].astype(jnp.bfloat16)
@@ -448,7 +462,7 @@
     width = query_weight.shape[1]
     return pl.pallas_call(
         functools.partial(layer_kernel, S, T, L, R),
-        out_shape=jax.ShapeDtypeStruct((R, D), bf),
+        out_shape=pltpu.VMEM((R, D), bf),
         in_specs=[hbm, hbm, hbm, hbm, hbm, smem, vmem],
         out_specs=vmem,
         scratch_shapes=[
@@ -603,7 +617,7 @@
     def layer(*args):
         L = args[5].shape[0] // T
         rows = args[0].shape[0] // (S * T)
-        fits = T == 4 and L == 2 and S == L * T and rows % 16 == 0
+        fits = T == 4 and L == 2 and S == L * T and rows % 16 == 0 and rows * 8 % 128 == 0
         local = functools.partial(fused, S, T, L) if fits else shards
         return jax.shard_map(
             local, mesh=mesh, in_specs=in_specs, out_specs=out_specs, check_vma=False

time: 64.6 us -> 61.3 us (0.949)
  the two profiles are of different devices: /device:TPU:25 before, /device:TPU:0 now
where the time goes in v3:
time: 61.3 us; the launch traced here: 60.9 us
  Pallas kernels  60.1 us (98%)
  local copies, waits for them, and re-layouts  0.77 us (1%)
    pallas_call x1, Pallas kernels, fused(): pl.pallas_call(functools.partial(layer_kernel, S, T, L, R), out_shape=plt...  60.1 us

profile of v3, /device:TPU:0, one launch (start us, length us, event | category | flops | bytes accessed | tf_op | source)
XLA Modules:
  0.0 60.9 jit_solution(1386537461061518715)
XLA Ops:
  0.0 60.1 %shard_map.73 = bf16[112,2048]{1,0:T(8,128)(2,1)S(1)} custom-call(bf16[112,2048]{1,0:T(8,128)(2,1)} %act.1, bf16[2048,512]{1,0:T(8,128)(2,1)} %qw.1, bf16[2048,512]{1,0:T(8,128)(2,1)} %kw.1, bf16[2048,512]{1,0:T(8,128)(2,1)} %vw.1, bf16[2,256,2048]{2,1,0:T(8,128)(2,1)} %bitcast.2, f32[2]{0:T(128)} %lam_in.1, f32[1,256]{1,0:T(1,128)} %bitcast.3), custom_call_target="tpu_custom_call" | custom-call | tf_op jit(solution)/shard_map/pallas_call | solution.py:463
  60.1 0.8 %copy.9 = bf16[112,2048]{1,0:T(8,128)(2,1)} copy(bf16[112,2048]{1,0:T(8,128)(2,1)S(1)} %shard_map.73) | data formatting | bytes 917504

commit v4 on v3

--- a/solution.py
+++ b/solution.py
@@ -21,7 +21,7 @@
     S, T, L, R,
     act, qw, kw, vw, ow, lam_in, gain,
     out,
-    A, WP, W, PR, PC, KV, HO, HI, LS, LB, ACC, MX, DN, TOT,
+    A, WP, W, PQ, PK, QC, KV, HO, HI, LS, LB, ACC, MX, DN, TOT,
     w_sem, own_sem, a_send, a_recv, lam_send, lam_recv,
     ox_send, ox_recv, oy_send, oy_recv, m_send, m_recv,
     p_send, p_recv, f_send, f_recv, h_send, h_recv,
@@ -99,14 +99,17 @@
         return W.at[owner * L + l, pl.ds(k * cut, cut)]
 
     def ow_across(k):
-        l, q = (side, order[k]) if k < 4 else (1 - side, 1)
+        l, q = (side, order[k]) if k < 4 else (1 - side, order[3])
         return remote(
             ow.at[l, pl.ds(q * cut, cut)], slab(t, l, q), ox_send.at[k], ox_recv.at[k], s, across
         )
 
     def ow_side(k, l):
-        part = slab(across, l, order[k])
-        target = beside if k == 2 else pair
+        if k < 2:
+            part = slab(across, l, order[k])
+        else:
+            part = W.at[across * L + l, pl.ds(order[2] * cut + (k - 2) * (cut // 2), cut // 2)]
+        target = (beside, pair)[k % 2]
         return remote(part, part, oy_send.at[k], oy_recv.at[k], target, t)
 
     def ow_pass(k):
@@ -146,67 +149,63 @@
     def piece_sp(l):
         return (c * L + l) * Y + y
 
-    def piece(l, xx, d):
+    def kv_rows(row, zs, xx, core):
+        return pl.ds(((zs * Y + row) * T + xx * 2 + core) * R, R)
+
+    def ends(kind, l, xx, d):
+        if kind == 0:
+            return PK.at[l, xx, d], KV.at[kv_rows(y, z, xx, d)]
+        return PQ.at[l, xx, d], QC.at[z, xx]
+
+    def piece(kind, l, xx, d):
         return remote(
-            PR.at[l, xx, d], PC.at[z, xx], p_send.at[l, xx, d], p_recv.at[z, xx],
+            *ends(kind, l, xx, d), p_send.at[kind, l, xx, d], p_recv.at[kind, z, xx],
             piece_sp(l), x * 2 + d,
         )
 
     def stays(l, d):
         return (piece_sp(l) == s) & (c == d)
 
-    def send_piece(l, xx, d):
-        @pl.when(stays(l, d))
-        def _():
-            pltpu.make_async_copy(PR.at[l, xx, d], PC.at[z, xx], p_recv.at[z, xx]).start()
-
-        @pl.when(jnp.logical_not(stays(l, d)))
-        def _():
-            piece(l, xx, d).start()
+    def send(kind, xx, i):
+        l = head_at(i)
+        for d in range(2):
+            @pl.when(stays(l, d))
+            def _():
+                pltpu.make_async_copy(*ends(kind, l, xx, d), p_recv.at[kind, z, xx]).start()
+
+            @pl.when(jnp.logical_not(stays(l, d)))
+            def _():
+                piece(kind, l, xx, d).start()
 
     def project(xx, i):
         l = head_at(i)
         rows = A[pl.ds(xx * 2, 2)].reshape(2 * R, A.shape[2])
         got = jnp.dot(rows, WP[l], preferred_element_type=jnp.float32)
-        PR[l, xx, :, :, :256] = (got[:, :256] * scale).astype(jnp.bfloat16).reshape(2, R, 256)
-        PR[l, xx, :, :, 256:] = got[:, 256:].astype(jnp.bfloat16).reshape(2, R, 512)
-
-    def send(xx, i):
-        for d in range(2):
-            send_piece(head_at(i), xx, d)
-
-    def kv_rows(row, zs, xx, core):
-        return pl.ds(((zs * Y + row) * T + xx * 2 + core) * R, R)
-
-    def kv_part(zs, xx):
-        return PC.at[zs, xx, :, 256:768]
+        PQ[l, xx] = (got[:, :256] * scale).astype(jnp.bfloat16).reshape(2, R, 256)
+        PK[l, xx] = got[:, 256:].astype(jnp.bfloat16).reshape(2, R, 512)
 
     def to_beside(zs, xx):
-        return remote(
-            kv_part(zs, xx), KV.at[kv_rows(y, zs, xx, c)],
-            f_send.at[0, zs, xx], f_recv.at[0, zs, xx], beside, t,
-        )
+        part = KV.at[kv_rows(y, zs, xx, c)]
+        return remote(part, part, f_send.at[0, zs, xx], f_recv.at[0, zs, xx], beside, t)
 
     def to_mate(zs, xx):
-        return remote(
-            kv_part(zs, xx), KV.at[kv_rows(y, zs, xx, c)],
-            f_send.at[1, zs, xx], f_recv.at[1, zs, xx], s, mate,
-        )
+        part = KV.at[kv_rows(y, zs, xx, c)]
+        return remote(part, part, f_send.at[1, zs, xx], f_recv.at[1, zs, xx], s, mate)
 
     def to_mate_again(zs, xx):
         part = KV.at[kv_rows(1 - y, zs, xx, c)]
         return remote(part, part, f_send.at[2, zs, xx], f_recv.at[2, zs, xx], s, mate)
 
-    def to_self(zs, xx):
-        return pltpu.make_async_copy(
-            kv_part(zs, xx), KV.at[kv_rows(y, zs, xx, c)], f_recv.at[3, zs, xx]
-        )
-
     def forward(zs, xx):
-        remote(PR.at[0, 0, 0], PC.at[zs, xx], p_send.at[0, 0, 0], p_recv.at[zs, xx], s, mate).wait_recv()
+        part = KV.at[kv_rows(y, zs, xx, c)]
+        remote(part, part, p_send.at[0, 0, 0, 0], p_recv.at[0, zs, xx], s, mate).wait_recv()
         to_beside(zs, xx).start()
         to_mate(zs, xx).start()
-        to_self(zs, xx).start()
+
+    def wait_q(zs):
+        for xx in range(X):
+            part = QC.at[zs, xx]
+            remote(part, part, p_send.at[1, 0, 0, 0], p_recv.at[1, zs, xx], s, mate).wait_recv()
 
     def relay(zs, xx):
         to_beside(zs, xx).wait_recv()
@@ -214,7 +213,6 @@
 
     def wait_plane(zs):
         for xx in range(X):
-            to_self(zs, xx).wait()
             to_mate(zs, xx).wait_recv()
             to_mate_again(zs, xx).wait_recv()
 
@@ -227,7 +225,7 @@
         ahead_by = row + jnp.where(row >= R, R, 0) - lane + (y * span + c * R + (i - j) * k_rows)
         cols = range(0, k_rows, 128)
         for m in range(2):
-            q = PC[i, :, :, m * 128:(m + 1) * 128].reshape(q_rows, 128)
+            q = QC[i, :, :, m * 128:(m + 1) * 128].reshape(q_rows, 128)
             keys = KV[pl.ds(j * k_rows, k_rows), m * 128:(m + 1) * 128]
             sc = lax.dot_general(
                 q, keys, (((1,), (1,)), ((), ())), preferred_element_type=jnp.float32
@@ -276,11 +274,13 @@
         weight_copy(0, part).wait()
     wait_act(mate)
     project(x, 0)
-    send(x, 0)
+    send(0, x, 0)
     for part in range(3):
         weight_copy(1, part).wait()
     project(x, 1)
-    send(x, 1)
+    send(0, x, 1)
+    for i in range(L):
+        send(1, x, i)
     forward(z, x)
     lam_out().start()
     ow_mate().start()
@@ -293,12 +293,17 @@
     act_pass().start()
     forward(later, x)
     wait_act(diagonal)
-    for i in range(L):
-        project(1 - x, i)
-
-        @pl.when(jnp.logical_not(held))
-        def _():
-            send(1 - x, i)
+    def send_rest():
+        for kind in range(2):
+            for i in range(L):
+                send(kind, 1 - x, i)
+
+    project(1 - x, 0)
+    project(1 - x, 1)
+
+    @pl.when(jnp.logical_not(held))
+    def _():
+        send_rest()
 
     forward(z, 1 - x)
     relay(early, x)
@@ -309,41 +314,56 @@
     after = jnp.where(top, near, third)
     forward(sooner, 1 - x)
 
-    @pl.when(held)
-    def _():
-        for i in range(L):
-            send(1 - x, i)
-
     relay(z, 1 - x)
     forward(after, 1 - x)
     relay(behind, x)
+
+    @pl.when(held)
+    def _():
+        send_rest()
+
     relay(sooner, 1 - x)
-    ow_across(0).wait_recv()
-    ow_side(0, side).start()
-    ow_pass(0).start()
-    ow_across(1).wait_recv()
-    ow_side(1, side).start()
-    ow_pass(1).start()
     lam_out().wait_recv()
+    wait_q(z)
+    wait_q(near)
+
+    @pl.when(top)
+    def _():
+        wait_q(third)
+
     wait_plane(z)
     wait_plane(sooner)
 
     def body_step(k, carry):
         upper = half == 1
 
-        @pl.when(k == 4 - half)
+        @pl.when(k == 0)
+        def _():
+            for n in range(2):
+                ow_across(n).wait_recv()
+                ow_pass(n).start()
+            ow_side(1, side).start()
+
+        @pl.when(k == 2)
+        def _():
+            ow_across(2).wait_recv()
+            ow_side(3, side).start()
+            ow_pass(2).start()
+
+        @pl.when(k == 3)
         def _():
             forward(last, 1 - x)
-
-        @pl.when(k == 3)
-        def _():
             relay(after, 1 - x)
-            ow_across(2).wait_recv()
-            ow_pass(2).start()
+
+            @pl.when(jnp.logical_not(top))
+            def _():
+                wait_q(third)
+
             wait_plane(after)
 
-        @pl.when(k == 5 - half)
-        def _():
+        @pl.when(k == 4)
+        def _():
+            ow_side(0, side).start()
             ow_side(2, side).start()
 
         n = k % 3
@@ -363,18 +383,26 @@
     lax.fori_loop(0, 6, body_step, 0)
 
     def last_step(k, carry):
-        @pl.when(k == 1 - half)
+        @pl.when(k == 0)
+        def _():
+            wait_q(last)
+
+        @pl.when(k == 2 - half)
         def _():
             relay(last, 1 - x)
 
-        @pl.when(k == 3 * (1 - half))
+        @pl.when(k == 3 - 2 * half)
         def _():
             wait_plane(last)
 
-        i = jnp.where((half == 0) | (k == 1) | (k == 2), last, jnp.where(k == 0, near, z))
-        chunk(i, jnp.where(half == 0, k, jnp.where(k == 1, 0, last)))
-
-        @pl.when(jnp.where(half == 0, k == 3, k != 1))
+        i = jnp.where(
+            k == 1, jnp.where(top, last, near),
+            jnp.where(k == 2, jnp.where(top, z, last), jnp.where(top, near, z)),
+        )
+        i = jnp.where((half == 0) | (k == 0), last, i)
+        chunk(i, jnp.where(half == 0, k, jnp.where(k == 0, 0, last)))
+
+        @pl.when(jnp.where(half == 0, k == 3, k > 0))
         def _():
             finish(i)
 
@@ -383,8 +411,11 @@
     lax.fori_loop(0, 4, last_step, 0)
     ow_across(3).wait_recv()
     ow_pass(3).start()
-    ow_side(0, 1 - side).wait_recv()
-    ow_pass(5).start()
+    for k in range(2):
+        ow_side(k, 1 - side).wait_recv()
+        ow_pass(5 + k).start()
+    ow_across(4).wait_recv()
+    ow_pass(4).start()
     act_across().wait_send()
     act_mate().wait_send()
     act_pass().wait_send()
@@ -395,7 +426,8 @@
             for d in range(2):
                 @pl.when(jnp.logical_not(stays(l, d)))
                 def _():
-                    piece(l, xx, d).wait_send()
+                    for kind in range(2):
+                        piece(kind, l, xx, d).wait_send()
 
     def settle(zs, carry):
         for xx in range(X):
@@ -410,29 +442,45 @@
     ow_mate().wait_recv()
     TOT[...] = jnp.zeros(TOT.shape, jnp.float32)
 
-    def add_head(i, carry):
+    def add_head(i, code):
         @pl.when(i == 2)
         def _():
-            ow_side(1, 1 - side).wait_recv()
-            ow_pass(6).start()
-            ow_across(4).wait_recv()
-            ow_pass(4).start()
-            ow_side(2, 1 - side).wait_recv()
+            for k in range(4):
+                ow_pass(k).wait_recv()
+
+        @pl.when(i == 4 - 2 * low)
+        def _():
+            for k in range(2, 4):
+                ow_side(k, 1 - side).wait_recv()
             ow_pass(7).start()
-            for k in range(8):
+
+        @pl.when(i == 6 - 3 * low)
+        def _():
+            for k in range(4, 8):
                 ow_pass(k).wait_recv()
 
-        tail = i // 4
-        plane = (1 - tail) * (i % 2) + tail * (Z - 1 - (i - 4) // 2)
-        h = ((x + (1 - tail) * (i // 2) + tail * i) % 2) * 2 * L + plane
+        plane, off = code % 8 // 2, code % 2
+        plane = plane // 2 * 2 + (plane + off * side) % 2
+        h = (x + off) % 2 * 2 * L + plane
         remote(HO.at[0, 0], HI.at[h], h_send.at[0, 0], h_recv.at[h], s, mate).wait_recv()
         TOT[...] += jnp.dot(HI[h], W[h], preferred_element_type=jnp.float32)
-        return carry
-
-    lax.fori_loop(0, T * L, add_head, 0)
+        return code // 8
+
+    orders = [
+        functools.reduce(lambda total, e: total * 8 + e, reversed(order), 0)
+        for order in (
+            (0, 2, 1, 6, 4, 5, 3, 7), (0, 2, 1, 3, 6, 4, 5, 7),
+            (0, 2, 1, 4, 6, 5, 3, 7), (6, 0, 1, 3, 2, 5, 7, 4),
+        )
+    ]
+    code = jnp.where(
+        half == 0, jnp.where(low == 0, orders[0], orders[1]),
+        jnp.where(low == 0, orders[2], orders[3]),
+    )
+    lax.fori_loop(0, T * L, add_head, code)
     for k in range(5):
         ow_across(k).wait_send()
-    for k in range(3):
+    for k in range(4):
         ow_side(k, side).wait_send()
     for k in range(8):
         ow_pass(k).wait_send()
@@ -469,8 +517,9 @@
             pltpu.VMEM((T, R, D), bf),
             pltpu.VMEM((L, D, 3 * width // L), bf),
             pltpu.VMEM((T * L, VALUE, D), bf),
-            pltpu.VMEM((L, X, 2, R, 768), bf),
-            pltpu.VMEM((Z, X, R, 768), bf),
+            pltpu.VMEM((L, X, 2, R, 256), bf),
+            pltpu.VMEM((L, X, 2, R, 512), bf),
+            pltpu.VMEM((Z, X, R, 256), bf),
             pltpu.VMEM((S * T * R, 512), bf),
             pltpu.VMEM((Z, X, R, VALUE), bf),
             pltpu.VMEM((T * L, R, VALUE), bf),
@@ -483,9 +532,9 @@
             dma((L, 3)), dma((2,)),
             dma((3,)), dma((T,)),
             dma((1,)), dma((1,)),
-            dma((5,)), dma((5,)), dma((3,)), dma((3,)), dma((9,)), dma((9,)),
-            dma((L, X, 2)), dma((Z, X)),
-            dma((3, Z, X)), dma((4, Z, X)),
+            dma((5,)), dma((5,)), dma((4,)), dma((4,)), dma((9,)), dma((9,)),
+            dma((2, L, X, 2)), dma((2, Z, X)),
+            dma((3, Z, X)), dma((3, Z, X)),
             dma((Z, X)), dma((T * L,)),
         ],
         compiler_params=pltpu.CompilerParams(

time: 61.3 us -> 56.5 us (0.922)
  Pallas kernels: 60.1 us -> 55.6 us
    pallas_call x1, Pallas kernels: 60.1 us -> 55.6 us  [fused(): pl.pallas_call(functools.partial(layer_kernel, S, T, L, R), out_shape=plt...]
where the time goes in v4:
time: 56.5 us; the launch traced here: 56.3 us
  Pallas kernels  55.6 us (98%)
  local copies, waits for them, and re-layouts  0.77 us (1%)
    pallas_call x1, Pallas kernels, fused(): pl.pallas_call(functools.partial(layer_kernel, S, T, L, R), out_shape=plt...  55.6 us

profile of v4, /device:TPU:0, one launch (start us, length us, event | category | flops | bytes accessed | tf_op | source)
XLA Modules:
  0.0 56.3 jit_solution(6370617678196208168)
XLA Ops:
  0.0 55.6 %shard_map.73 = bf16[112,2048]{1,0:T(8,128)(2,1)S(1)} custom-call(bf16[112,2048]{1,0:T(8,128)(2,1)} %act.1, bf16[2048,512]{1,0:T(8,128)(2,1)} %qw.1, bf16[2048,512]{1,0:T(8,128)(2,1)} %kw.1, bf16[2048,512]{1,0:T(8,128)(2,1)} %vw.1, bf16[2,256,2048]{2,1,0:T(8,128)(2,1)} %bitcast.2, f32[2]{0:T(128)} %lam_in.1, f32[1,256]{1,0:T(1,128)} %bitcast.3), custom_call_target="tpu_custom_call" | custom-call | tf_op jit(solution)/shard_map/pallas_call | solution.py:511
  55.6 0.8 %copy.9 = bf16[112,2048]{1,0:T(8,128)(2,1)} copy(bf16[112,2048]{1,0:T(8,128)(2,1)S(1)} %shard_map.73) | data formatting | bytes 917504

commit v5 on v4

--- a/solution.py
+++ b/solution.py
@@ -19,12 +19,12 @@
 
 def layer_kernel(
     S, T, L, R,
-    act, qw, kw, vw, ow, lam_in, gain,
+    act, qw, kw, vw, ow, lam_ref, gain_ref,
     out,
-    A, WP, W, PQ, PK, QC, KV, HO, HI, LS, LB, ACC, MX, DN, TOT,
+    lam_in, gain, A, WP, W, PQ, PK, QC, KV, HO, HI, LS, LB, ACC, MX, DN, TOT,
     w_sem, own_sem, a_send, a_recv, lam_send, lam_recv,
     ox_send, ox_recv, oy_send, oy_recv, m_send, m_recv,
-    p_send, p_recv, f_send, f_recv, h_send, h_recv,
+    p_send, p_recv, q_recv, f_send, f_recv, g_recv, h_send, h_recv,
 ):
     X, Y = 2, 2
     Z = S // Y
@@ -71,12 +71,16 @@
         l = head_at(i)
         return pltpu.make_async_copy(
             (qw, kw, vw)[part].at[:, pl.ds(pl.multiple_of(l * 256, 256), 256)],
-            WP.at[l, :, part * 256:(part + 1) * 256], w_sem.at[i, part],
+            WP.at[l, :, part * 256:(part + 1) * 256], w_sem.at[i],
         )
 
     def own_act():
         return pltpu.make_async_copy(act, A.at[t], own_sem.at[0])
 
+    def small(k):
+        pair = ((lam_ref, lam_in), (gain_ref, gain))[k]
+        return pltpu.make_async_copy(*pair, own_sem.at[2 + k])
+
     def own_ow():
         return pltpu.make_async_copy(ow, W.at[pl.ds(t * L, L)], own_sem.at[1])
 
@@ -84,10 +88,10 @@
         return remote(A.at[t], A.at[t], a_send.at[0], a_recv.at[t], s, across)
 
     def act_mate():
-        return remote(A.at[t], A.at[t], a_send.at[1], a_recv.at[t], s, mate)
+        return remote(A.at[t], A.at[t], a_send.at[0], a_recv.at[t], s, mate)
 
     def act_pass():
-        return remote(A.at[across], A.at[across], a_send.at[2], a_recv.at[across], s, mate)
+        return remote(A.at[across], A.at[across], a_send.at[0], a_recv.at[across], s, mate)
 
     def wait_act(i):
         remote(A.at[i], A.at[i], a_send.at[0], a_recv.at[i], s, mate).wait_recv()
@@ -101,7 +105,7 @@
     def ow_across(k):
         l, q = (side, order[k]) if k < 4 else (1 - side, order[3])
         return remote(
-            ow.at[l, pl.ds(q * cut, cut)], slab(t, l, q), ox_send.at[k], ox_recv.at[k], s, across
+            ow.at[l, pl.ds(q * cut, cut)], slab(t, l, q), ox_send.at[0], ox_recv.at[k], s, across
         )
 
     def ow_side(k, l):
@@ -110,31 +114,31 @@
         else:
             part = W.at[across * L + l, pl.ds(order[2] * cut + (k - 2) * (cut // 2), cut // 2)]
         target = (beside, pair)[k % 2]
-        return remote(part, part, oy_send.at[k], oy_recv.at[k], target, t)
+        return remote(part, part, oy_send.at[0], oy_recv.at[min(k, 2)], target, t)
 
     def ow_pass(k):
         l, q = (side, order[k]) if k < 4 else (1 - side, (1, 0, 2, 3)[k - 4])
         part = slab(across, l, q)
-        return remote(part, part, m_send.at[k], m_recv.at[k], s, mate)
+        return remote(part, part, m_send.at[0], m_recv.at[k // 4], s, mate)
 
     def ow_mate():
-        return remote(ow, W.at[pl.ds(t * L, L)], m_send.at[8], m_recv.at[8], s, mate)
+        return remote(ow, W.at[pl.ds(t * L, L)], m_send.at[0], m_recv.at[2], s, mate)
 
     def lam_out():
         return remote(LS, LB, lam_send.at[0], lam_recv.at[0], s, mate)
 
     barrier = pltpu.get_barrier_semaphore()
     own_act().start()
-    for part in range(3):
-        weight_copy(0, part).start()
+    small(0).start()
+    small(1).start()
     greeted = [(beside, t)]
     for i in range(Z):
         row = ((z + i) % Z) * Y + y
         greeted += [(row, mate), (row, across)] + ([(row, t)] if i > 0 else [])
     for sp, tp in greeted:
         pl.semaphore_signal(barrier, inc=1, device_id=(sp, tp), device_id_type=MESH)
-    for l in range(L):
-        LS[l] = jnp.full((8, 128), lam_in[l], jnp.float32)
+    for part in range(3):
+        weight_copy(0, part).start()
     own_act().wait()
     for part in range(3):
         weight_copy(1, part).start()
@@ -143,6 +147,10 @@
 
     act_across().start()
     act_mate().start()
+    small(0).wait()
+    small(1).wait()
+    for l in range(L):
+        LS[l] = jnp.full((8, 128), lam_in[l], jnp.float32)
     for k in range(5):
         ow_across(k).start()
 
@@ -157,9 +165,12 @@
             return PK.at[l, xx, d], KV.at[kv_rows(y, z, xx, d)]
         return PQ.at[l, xx, d], QC.at[z, xx]
 
+    def arrival(kind, zs, xx):
+        return p_recv.at[zs, xx] if kind == 0 else q_recv.at[zs]
+
     def piece(kind, l, xx, d):
         return remote(
-            *ends(kind, l, xx, d), p_send.at[kind, l, xx, d], p_recv.at[kind, z, xx],
+            *ends(kind, l, xx, d), p_send.at[kind], arrival(kind, z, xx),
             piece_sp(l), x * 2 + d,
         )
 
@@ -171,7 +182,7 @@
         for d in range(2):
             @pl.when(stays(l, d))
             def _():
-                pltpu.make_async_copy(*ends(kind, l, xx, d), p_recv.at[kind, z, xx]).start()
+                pltpu.make_async_copy(*ends(kind, l, xx, d), arrival(kind, z, xx)).start()
 
             @pl.when(jnp.logical_not(stays(l, d)))
             def _():
@@ -186,35 +197,33 @@
 
     def to_beside(zs, xx):
         part = KV.at[kv_rows(y, zs, xx, c)]
-        return remote(part, part, f_send.at[0, zs, xx], f_recv.at[0, zs, xx], beside, t)
+        return remote(part, part, f_send.at[0], f_recv.at[zs, xx], beside, t)
 
     def to_mate(zs, xx):
         part = KV.at[kv_rows(y, zs, xx, c)]
-        return remote(part, part, f_send.at[1, zs, xx], f_recv.at[1, zs, xx], s, mate)
+        return remote(part, part, f_send.at[0], g_recv.at[zs], s, mate)
 
     def to_mate_again(zs, xx):
         part = KV.at[kv_rows(1 - y, zs, xx, c)]
-        return remote(part, part, f_send.at[2, zs, xx], f_recv.at[2, zs, xx], s, mate)
+        return remote(part, part, f_send.at[0], g_recv.at[zs], s, mate)
 
     def forward(zs, xx):
         part = KV.at[kv_rows(y, zs, xx, c)]
-        remote(part, part, p_send.at[0, 0, 0, 0], p_recv.at[0, zs, xx], s, mate).wait_recv()
+        remote(part, part, p_send.at[0], p_recv.at[zs, xx], s, mate).wait_recv()
         to_beside(zs, xx).start()
         to_mate(zs, xx).start()
 
     def wait_q(zs):
-        for xx in range(X):
-            part = QC.at[zs, xx]
-            remote(part, part, p_send.at[1, 0, 0, 0], p_recv.at[1, zs, xx], s, mate).wait_recv()
+        part = QC.at[zs]
+        remote(part, part, p_send.at[1], q_recv.at[zs], s, mate).wait_recv()
 
     def relay(zs, xx):
         to_beside(zs, xx).wait_recv()
         to_mate_again(zs, xx).start()
 
     def wait_plane(zs):
-        for xx in range(X):
-            to_mate(zs, xx).wait_recv()
-            to_mate_again(zs, xx).wait_recv()
+        part = KV.at[pl.ds(0, 2 * X * R)]
+        remote(part, part, f_send.at[0], g_recv.at[zs], s, mate).wait_recv()
 
     q_rows = X * R
     k_rows = Y * span
@@ -224,6 +233,7 @@
         lane = lax.broadcasted_iota(jnp.int32, (q_rows, 128), 1)
         ahead_by = row + jnp.where(row >= R, R, 0) - lane + (y * span + c * R + (i - j) * k_rows)
         cols = range(0, k_rows, 128)
+        weights, factors = [], []
         for m in range(2):
             q = QC[i, :, :, m * 128:(m + 1) * 128].reshape(q_rows, 128)
             keys = KV[pl.ds(j * k_rows, k_rows), m * 128:(m + 1) * 128]
@@ -238,15 +248,20 @@
             factor = jnp.exp2(old - new)
             DN[i, m] = DN[i, m] * factor + functools.reduce(jnp.add, parts)
             MX[i, m] = new
-            p = jnp.concatenate([part.astype(jnp.bfloat16) for part in parts], axis=1)
-            values = KV[pl.ds(j * k_rows, k_rows), 256:512]
-            got = jnp.dot(p, values, preferred_element_type=jnp.float32)
+            weights.append(jnp.concatenate([part.astype(jnp.bfloat16) for part in parts], axis=1))
+            factors.append(factor)
+        values = KV[pl.ds(j * k_rows, k_rows), 256:512]
+        got = jnp.dot(
+            jnp.concatenate(weights, axis=0), values, preferred_element_type=jnp.float32
+        )
+        for m in range(2):
             for b in range(0, VALUE, 128):
-                ACC[i, m, :, b:b + 128] = ACC[i, m, :, b:b + 128] * factor + got[:, b:b + 128]
+                fresh = got[m * q_rows:(m + 1) * q_rows, b:b + 128]
+                ACC[i, m, :, b:b + 128] = ACC[i, m, :, b:b + 128] * factors[m] + fresh
 
     def home(zs, xx):
         return remote(
-            HO.at[zs, xx], HI.at[head], h_send.at[zs, xx], h_recv.at[head],
+            HO.at[zs, xx], HI.at[head], h_send.at[0], h_recv.at[head],
             zs * Y + y, xx * 2 + c,
         )
 
@@ -270,13 +285,14 @@
             def _():
                 home(i, xx).start()
 
-    for part in range(3):
-        weight_copy(0, part).wait()
+    def wait_weights(i):
+        pltpu.make_async_copy(WP.at[i], WP.at[i], w_sem.at[i]).wait()
+
+    wait_weights(0)
     wait_act(mate)
     project(x, 0)
     send(0, x, 0)
-    for part in range(3):
-        weight_copy(1, part).wait()
+    wait_weights(1)
     project(x, 1)
     send(0, x, 1)
     for i in range(L):
@@ -397,7 +413,7 @@
 
         i = jnp.where(
             k == 1, jnp.where(top, last, near),
-            jnp.where(k == 2, jnp.where(top, z, last), jnp.where(top, near, z)),
+            jnp.where(k == 2, jnp.where(top, near, last), z),
         )
         i = jnp.where((half == 0) | (k == 0), last, i)
         chunk(i, jnp.where(half == 0, k, jnp.where(k == 0, 0, last)))
@@ -416,53 +432,53 @@
         ow_pass(5 + k).start()
     ow_across(4).wait_recv()
     ow_pass(4).start()
-    act_across().wait_send()
-    act_mate().wait_send()
-    act_pass().wait_send()
-    ow_mate().wait_send()
+    def sent(part, sem):
+        remote(part, part, sem, lam_recv.at[0], s, mate).wait_send()
+
+    sent(A.at[pl.ds(0, 3)], a_send.at[0])
     lam_out().wait_send()
-    for l in range(L):
-        for xx in range(X):
-            for d in range(2):
-                @pl.when(jnp.logical_not(stays(l, d)))
-                def _():
-                    for kind in range(2):
-                        piece(kind, l, xx, d).wait_send()
-
-    def settle(zs, carry):
-        for xx in range(X):
-            to_beside(zs, xx).wait_send()
-            to_mate(zs, xx).wait_send()
-            to_mate_again(zs, xx).wait_send()
-
-        return carry
-
-    lax.fori_loop(0, Z, settle, 0)
+    sent(KV.at[pl.ds(0, 3 * Z * X * R)], f_send.at[0])
+    keeps = c == half
+
+    def sent_pieces(count):
+        sent(KV.at[pl.ds(0, count * X * R)], p_send.at[0])
+        sent(QC.at[pl.ds(0, count)], p_send.at[1])
+
+    @pl.when(keeps)
+    def _():
+        sent_pieces(2 * L - 1)
+
+    @pl.when(jnp.logical_not(keeps))
+    def _():
+        sent_pieces(2 * L)
+
     own_ow().wait()
     ow_mate().wait_recv()
     TOT[...] = jnp.zeros(TOT.shape, jnp.float32)
 
+    def wait_passed(n):
+        part = W.at[0]
+        remote(part, part, m_send.at[0], m_recv.at[n], s, mate).wait_recv()
+
     def add_head(i, code):
         @pl.when(i == 2)
         def _():
-            for k in range(4):
-                ow_pass(k).wait_recv()
+            wait_passed(0)
 
         @pl.when(i == 4 - 2 * low)
         def _():
-            for k in range(2, 4):
-                ow_side(k, 1 - side).wait_recv()
+            part = slab(across, 0, 0)
+            remote(part, part, oy_send.at[0], oy_recv.at[2], s, mate).wait_recv()
             ow_pass(7).start()
 
         @pl.when(i == 6 - 3 * low)
         def _():
-            for k in range(4, 8):
-                ow_pass(k).wait_recv()
+            wait_passed(1)
 
         plane, off = code % 8 // 2, code % 2
         plane = plane // 2 * 2 + (plane + off * side) % 2
         h = (x + off) % 2 * 2 * L + plane
-        remote(HO.at[0, 0], HI.at[h], h_send.at[0, 0], h_recv.at[h], s, mate).wait_recv()
+        remote(HO.at[0, 0], HI.at[h], h_send.at[0], h_recv.at[h], s, mate).wait_recv()
         TOT[...] += jnp.dot(HI[h], W[h], preferred_element_type=jnp.float32)
         return code // 8
 
@@ -478,24 +494,13 @@
         jnp.where(low == 0, orders[2], orders[3]),
     )
     lax.fori_loop(0, T * L, add_head, code)
-    for k in range(5):
-        ow_across(k).wait_send()
-    for k in range(4):
-        ow_side(k, side).wait_send()
-    for k in range(8):
-        ow_pass(k).wait_send()
+    sent(W.at[pl.ds(0, 5), pl.ds(0, cut)], ox_send.at[0])
+    sent(W.at[0, pl.ds(0, 3 * cut)], oy_send.at[0])
+    sent(W.at[pl.ds(0, 2 * L)], m_send.at[0])
     out[...] = TOT[...].astype(jnp.bfloat16)
 
 
-    def drain(zs, carry):
-        for xx in range(X):
-            @pl.when(jnp.logical_not(ends_here(zs, xx)))
-            def _():
-                home(zs, xx).wait_send()
-
-        return carry
-
-    lax.fori_loop(0, Z, drain, 0)
+    sent(HI.at[pl.ds(0, Z * X - 1)], h_send.at[0])
 
 
 def fused(S, T, L, activations, query_weight, key_weight, value_weight, out_weight, lambdas, head_gain):
@@ -505,15 +510,16 @@
     bf, f32 = jnp.bfloat16, jnp.float32
     vmem = pl.BlockSpec(memory_space=pltpu.VMEM)
     hbm = pl.BlockSpec(memory_space=pl.ANY)
-    smem = pl.BlockSpec(memory_space=pltpu.SMEM)
     dma = pltpu.SemaphoreType.DMA
     width = query_weight.shape[1]
     return pl.pallas_call(
         functools.partial(layer_kernel, S, T, L, R),
         out_shape=pltpu.VMEM((R, D), bf),
-        in_specs=[hbm, hbm, hbm, hbm, hbm, smem, vmem],
+        in_specs=[hbm] * 7,
         out_specs=vmem,
         scratch_shapes=[
+            pltpu.SMEM((L,), f32),
+            pltpu.VMEM((1, VALUE), f32),
             pltpu.VMEM((T, R, D), bf),
             pltpu.VMEM((L, D, 3 * width // L), bf),
             pltpu.VMEM((T * L, VALUE, D), bf),
@@ -529,13 +535,13 @@
             pltpu.VMEM((Z, 2, X * R, 128), f32),
             pltpu.VMEM((Z, 2, X * R, 128), f32),
             pltpu.VMEM((R, D), f32),
-            dma((L, 3)), dma((2,)),
-            dma((3,)), dma((T,)),
+            dma((L,)), dma((4,)),
+            dma((1,)), dma((T,)),
             dma((1,)), dma((1,)),
-            dma((5,)), dma((5,)), dma((4,)), dma((4,)), dma((9,)), dma((9,)),
-            dma((2, L, X, 2)), dma((2, Z, X)),
-            dma((3, Z, X)), dma((3, Z, X)),
-            dma((Z, X)), dma((T * L,)),
+            dma((1,)), dma((5,)), dma((1,)), dma((3,)), dma((1,)), dma((3,)),
+            dma((2,)), dma((Z, X)), dma((Z,)),
+            dma((1,)), dma((Z, X)), dma((Z,)),
+            dma((1,)), dma((T * L,)),
         ],
         compiler_params=pltpu.CompilerParams(
             has_side_effects=True, collective_id=0, vmem_limit_bytes=60 * 1024 * 1024

time: 56.5 us -> 54.4 us (0.963)
  Pallas kernels: 55.6 us -> 53.4 us
    pallas_call x1, Pallas kernels: 55.6 us -> 53.4 us  [fused(): pl.pallas_call(functools.partial(layer_kernel, S, T, L, R), out_shape=plt...]
where the time goes in v5:
time: 54.4 us; the launch traced here: 54.2 us
  Pallas kernels  53.4 us (98%)
  local copies, waits for them, and re-layouts  0.77 us (1%)
    pallas_call x1, Pallas kernels, fused(): pl.pallas_call(functools.partial(layer_kernel, S, T, L, R), out_shape=plt...  53.4 us

profile of v5, /device:TPU:0, one launch (start us, length us, event | category | flops | bytes accessed | tf_op | source)
XLA Modules:
  0.0 54.2 jit_solution(8361567974680841977)
XLA Ops:
  0.0 53.4 %shard_map.73 = bf16[112,2048]{1,0:T(8,128)(2,1)S(1)} custom-call(bf16[112,2048]{1,0:T(8,128)(2,1)} %act.1, bf16[2048,512]{1,0:T(8,128)(2,1)} %qw.1, bf16[2048,512]{1,0:T(8,128)(2,1)} %kw.1, bf16[2048,512]{1,0:T(8,128)(2,1)} %vw.1, bf16[2,256,2048]{2,1,0:T(8,128)(2,1)} %bitcast.2, f32[2]{0:T(128)} %lam_ref.1, f32[1,256]{1,0:T(1,128)} %bitcast.3), custom_call_target="tpu_custom_call" | custom-call | tf_op jit(solution)/shard_map/pallas_call | solution.py:515
  53.4 0.8 %copy.9 = bf16[112,2048]{1,0:T(8,128)(2,1)} copy(bf16[112,2048]{1,0:T(8,128)(2,1)S(1)} %shard_map.73) | data formatting | bytes 917504

commit v6 on v5

--- a/solution.py
+++ b/solution.py
@@ -108,12 +108,12 @@
             ow.at[l, pl.ds(q * cut, cut)], slab(t, l, q), ox_send.at[0], ox_recv.at[k], s, across
         )
 
-    def ow_side(k, l):
+    def ow_side(k, l, aside=False):
         if k < 2:
             part = slab(across, l, order[k])
         else:
             part = W.at[across * L + l, pl.ds(order[2] * cut + (k - 2) * (cut // 2), cut // 2)]
-        target = (beside, pair)[k % 2]
+        target = beside if aside else (beside, pair)[k % 2]
         return remote(part, part, oy_send.at[0], oy_recv.at[min(k, 2)], target, t)
 
     def ow_pass(k):
@@ -315,11 +315,18 @@
                 send(kind, 1 - x, i)
 
     project(1 - x, 0)
-    project(1 - x, 1)
 
     @pl.when(jnp.logical_not(held))
     def _():
-        send_rest()
+        send(0, 1 - x, 0)
+
+    project(1 - x, 1)
+
+    @pl.when(jnp.logical_not(held))
+    def _():
+        send(0, 1 - x, 1)
+        for i in range(L):
+            send(1, 1 - x, i)
 
     forward(z, 1 - x)
     relay(early, x)
@@ -363,12 +370,18 @@
         @pl.when(k == 2)
         def _():
             ow_across(2).wait_recv()
-            ow_side(3, side).start()
             ow_pass(2).start()
 
+            @pl.when(z != 1)
+            def _():
+                ow_side(3, side).start()
+
+        @pl.when(k == 3 - 2 * top.astype(jnp.int32))
+        def _():
+            forward(last, 1 - x)
+
         @pl.when(k == 3)
         def _():
-            forward(last, 1 - x)
             relay(after, 1 - x)
 
             @pl.when(jnp.logical_not(top))
@@ -377,10 +390,14 @@
 
             wait_plane(after)
 
-        @pl.when(k == 4)
+        @pl.when(k == jnp.where(z == 0, 3, 4))
         def _():
             ow_side(0, side).start()
             ow_side(2, side).start()
+
+            @pl.when(z == 0)
+            def _():
+                ow_side(3, side, True).start()
 
         n = k % 3
         local = (k < 3) != top
@@ -460,42 +477,52 @@
         part = W.at[0]
         remote(part, part, m_send.at[0], m_recv.at[n], s, mate).wait_recv()
 
-    def add_head(i, code):
+    def add_head(i, carry):
+        entry = 0
+        for n in range(T * L):
+            entry = jnp.where(i == n, by_plane([order[n] for order in orders]), entry)
+
         @pl.when(i == 2)
         def _():
             wait_passed(0)
 
-        @pl.when(i == 4 - 2 * low)
+        @pl.when(i == pass_at)
         def _():
             part = slab(across, 0, 0)
             remote(part, part, oy_send.at[0], oy_recv.at[2], s, mate).wait_recv()
             ow_pass(7).start()
 
-        @pl.when(i == 6 - 3 * low)
+        @pl.when(i == late_at)
         def _():
             wait_passed(1)
 
-        plane, off = code % 8 // 2, code % 2
-        plane = plane // 2 * 2 + (plane + off * side) % 2
+        plane, off = entry // 4, entry // 2 % 2
+        plane = plane // 2 * 2 + (plane + entry % 2 * side) % 2
         h = (x + off) % 2 * 2 * L + plane
         remote(HO.at[0, 0], HI.at[h], h_send.at[0], h_recv.at[h], s, mate).wait_recv()
         TOT[...] += jnp.dot(HI[h], W[h], preferred_element_type=jnp.float32)
-        return code // 8
-
-    orders = [
-        functools.reduce(lambda total, e: total * 8 + e, reversed(order), 0)
-        for order in (
-            (0, 2, 1, 6, 4, 5, 3, 7), (0, 2, 1, 3, 6, 4, 5, 7),
-            (0, 2, 1, 4, 6, 5, 3, 7), (6, 0, 1, 3, 2, 5, 7, 4),
-        )
-    ]
-    code = jnp.where(
-        half == 0, jnp.where(low == 0, orders[0], orders[1]),
-        jnp.where(low == 0, orders[2], orders[3]),
+        return carry
+
+    def by_plane(values):
+        return jnp.where(
+            half == 0, jnp.where(low == 0, values[0], values[1]),
+            jnp.where(low == 0, values[2], values[3]),
+        )
+
+    pass_at = by_plane((4, 2, 4, 1))
+    late_at = by_plane((6, 3, 4, 3))
+    orders = (
+        (0, 4, 3, 12, 8, 11, 7, 15), (0, 4, 3, 7, 8, 10, 12, 14),
+        (0, 4, 3, 8, 7, 10, 12, 14), (12, 0, 3, 7, 4, 11, 15, 8),
     )
-    lax.fori_loop(0, T * L, add_head, code)
+    lax.fori_loop(0, T * L, add_head, 0)
     sent(W.at[pl.ds(0, 5), pl.ds(0, cut)], ox_send.at[0])
-    sent(W.at[0, pl.ds(0, 3 * cut)], oy_send.at[0])
+
+    for when, halves in ((z == 0, 7), (z == 1, 5), (z > 1, 6)):
+        @pl.when(when)
+        def _():
+            sent(W.at[0, pl.ds(0, halves * cut // 2)], oy_send.at[0])
+
     sent(W.at[pl.ds(0, 2 * L)], m_send.at[0])
     out[...] = TOT[...].astype(jnp.bfloat16)
 

time: 54.4 us -> 54.8 us (level)
  no operation moved by 1% of the time
where the time goes in v6:
time: 54.8 us; the launch traced here: 54.3 us
  Pallas kernels  53.5 us (98%)
  local copies, waits for them, and re-layouts  0.77 us (1%)
    pallas_call x1, Pallas kernels, fused(): pl.pallas_call(functools.partial(layer_kernel, S, T, L, R), out_shape=plt...  53.5 us

profile of v6, /device:TPU:0, one launch (start us, length us, event | category | flops | bytes accessed | tf_op | source)
XLA Modules:
  0.0 54.3 jit_solution(3259685152100303346)
XLA Ops:
  0.0 53.5 %shard_map.73 = bf16[112,2048]{1,0:T(8,128)(2,1)S(1)} custom-call(bf16[112,2048]{1,0:T(8,128)(2,1)} %act.1, bf16[2048,512]{1,0:T(8,128)(2,1)} %qw.1, bf16[2048,512]{1,0:T(8,128)(2,1)} %kw.1, bf16[2048,512]{1,0:T(8,128)(2,1)} %vw.1, bf16[2,256,2048]{2,1,0:T(8,128)(2,1)} %bitcast.2, f32[2]{0:T(128)} %lam_ref.1, f32[1,256]{1,0:T(1,128)} %bitcast.3), custom_call_target="tpu_custom_call" | custom-call | tf_op jit(solution)/shard_map/pallas_call | solution.py:542
  53.6 0.8 %copy.9 = bf16[112,2048]{1,0:T(8,128)(2,1)} copy(bf16[112,2048]{1,0:T(8,128)(2,1)S(1)} %shard_map.73) | data formatting | bytes 917504

commit v7 on v6

--- a/solution.py
+++ b/solution.py
@@ -372,6 +372,10 @@
             ow_across(2).wait_recv()
             ow_pass(2).start()
 
+            @pl.when(jnp.logical_not(top))
+            def _():
+                ow_side(2, side).start()
+
             @pl.when(z != 1)
             def _():
                 ow_side(3, side).start()
@@ -393,7 +397,10 @@
         @pl.when(k == jnp.where(z == 0, 3, 4))
         def _():
             ow_side(0, side).start()
-            ow_side(2, side).start()
+
+            @pl.when(top)
+            def _():
+                ow_side(2, side).start()
 
             @pl.when(z == 0)
             def _():
@@ -509,11 +516,11 @@
             jnp.where(low == 0, values[2], values[3]),
         )
 
-    pass_at = by_plane((4, 2, 4, 1))
-    late_at = by_plane((6, 3, 4, 3))
+    pass_at = by_plane((0, 1, 1, 1))
+    late_at = by_plane((6, 3, 4, 2))
     orders = (
         (0, 4, 3, 12, 8, 11, 7, 15), (0, 4, 3, 7, 8, 10, 12, 14),
-        (0, 4, 3, 8, 7, 10, 12, 14), (12, 0, 3, 7, 4, 11, 15, 8),
+        (0, 4, 3, 8, 7, 10, 12, 14), (12, 0, 14, 2, 4, 6, 10, 8),
     )
     lax.fori_loop(0, T * L, add_head, 0)
     sent(W.at[pl.ds(0, 5), pl.ds(0, cut)], ox_send.at[0])

time: 54.8 us -> 54.4 us (level)
  no operation moved by 1% of the time
where the time goes in v7:
time: 54.4 us; the launch traced here: 54.2 us
  Pallas kernels  53.4 us (98%)
  local copies, waits for them, and re-layouts  0.77 us (1%)
    pallas_call x1, Pallas kernels, fused(): pl.pallas_call(functools.partial(layer_kernel, S, T, L, R), out_shape=plt...  53.4 us

profile of v7, /device:TPU:0, one launch (start us, length us, event | category | flops | bytes accessed | tf_op | source)
XLA Modules:
  0.0 54.2 jit_solution(2949496052643771727)
XLA Ops:
  0.0 53.4 %shard_map.73 = bf16[112,2048]{1,0:T(8,128)(2,1)S(1)} custom-call(bf16[112,2048]{1,0:T(8,128)(2,1)} %act.1, bf16[2048,512]{1,0:T(8,128)(2,1)} %qw.1, bf16[2048,512]{1,0:T(8,128)(2,1)} %kw.1, bf16[2048,512]{1,0:T(8,128)(2,1)} %vw.1, bf16[2,256,2048]{2,1,0:T(8,128)(2,1)} %bitcast.2, f32[2]{0:T(128)} %lam_ref.1, f32[1,256]{1,0:T(1,128)} %bitcast.3), custom_call_target="tpu_custom_call" | custom-call | tf_op jit(solution)/shard_map/pallas_call | solution.py:549
  53.4 0.8 %copy.9 = bf16[112,2048]{1,0:T(8,128)(2,1)} copy(bf16[112,2048]{1,0:T(8,128)(2,1)S(1)} %shard_map.73) | data formatting | bytes 917504

commit v8 on v7

--- a/solution.py
+++ b/solution.py
@@ -339,11 +339,11 @@
 
     relay(z, 1 - x)
     forward(after, 1 - x)
-    relay(behind, x)
-
     @pl.when(held)
     def _():
         send_rest()
+
+    relay(behind, x)
 
     relay(sooner, 1 - x)
     lam_out().wait_recv()

time: 54.4 us -> 54.1 us (level)
  no operation moved by 1% of the time
where the time goes in v8:
time: 54.1 us; the launch traced here: 54 us
  Pallas kernels  53.2 us (98%)
  local copies, waits for them, and re-layouts  0.77 us (1%)
    pallas_call x1, Pallas kernels, fused(): pl.pallas_call(functools.partial(layer_kernel, S, T, L, R), out_shape=plt...  53.2 us

profile of v8, /device:TPU:0, one launch (start us, length us, event | category | flops | bytes accessed | tf_op | source)
XLA Modules:
  0.0 54.0 jit_solution(525886692149601587)
XLA Ops:
  0.0 53.2 %shard_map.73 = bf16[112,2048]{1,0:T(8,128)(2,1)S(1)} custom-call(bf16[112,2048]{1,0:T(8,128)(2,1)} %act.1, bf16[2048,512]{1,0:T(8,128)(2,1)} %qw.1, bf16[2048,512]{1,0:T(8,128)(2,1)} %kw.1, bf16[2048,512]{1,0:T(8,128)(2,1)} %vw.1, bf16[2,256,2048]{2,1,0:T(8,128)(2,1)} %bitcast.2, f32[2]{0:T(128)} %lam_ref.1, f32[1,256]{1,0:T(1,128)} %bitcast.3), custom_call_target="tpu_custom_call" | custom-call | tf_op jit(solution)/shard_map/pallas_call | solution.py:549
  53.2 0.8 %copy.9 = bf16[112,2048]{1,0:T(8,128)(2,1)} copy(bf16[112,2048]{1,0:T(8,128)(2,1)S(1)} %shard_map.73) | data formatting | bytes 917504
